TPU v7x, 32 devices: a whole 2x2x4 slice. The times are simulated.
32 devices in a mesh: ep: 8 (over z, y), tp: 4 (over x, core).
Axes of the slice: x: 2, y: 2, z: 4, core: 2. Of those that a mesh axis runs over, the one named last changes fastest.
Arguments:
- hidden: bfloat16 [256, 2048], P('ep')
- norm_gains: float32 [4, 2048], replicated, may hold values from 0.1 to 1.9
- w_query: bfloat16 [2048, 1024], P(None, 'tp'), may hold values from -0.125 to 0.125
- w_key: bfloat16 [2048, 1024], P(None, 'tp'), may hold values from -0.125 to 0.125
- w_value: bfloat16 [2048, 1024], P(None, 'tp'), may hold values from -0.125 to 0.125
- w_outgate: bfloat16 [2048, 1024], P(None, 'tp'), may hold values from -0.125 to 0.125
- w_input_gate: bfloat16 [2048, 8], replicated, may hold values from -0.125 to 0.125
- w_forget_gate: bfloat16 [2048, 8], replicated, may hold values from -0.125 to 0.125
- forget_bias: float32 [8], replicated, may hold values from -1 to 4
- w_mix_out: bfloat16 [1024, 2048], P('tp')
- state_matrix: float32 [256, 8, 128, 128], P('ep', 'tp'), may hold values from -0.6 to 0.6
- state_norm: float32 [256, 8, 128], P('ep', 'tp'), may hold values from -0.6 to 0.6
- state_max: float32 [256, 8], P('ep', 'tp'), may hold values from -4 to 4
- routes: int32 [256, 2], P('ep'), may hold values from 0 to 7, all different within a row; in each aligned block of 32 rows (0 to 31, 32 to 63, ...) at most 16 rows name the same one
- route_scores: float32 [256, 2], P('ep'), may hold values from 0.1 to 1
- expert_gate: bfloat16 [8, 2048, 3584], P('ep', None, 'tp'), may hold values from -0.125 to 0.125
- expert_up: bfloat16 [8, 2048, 3584], P('ep', None, 'tp'), may hold values from -0.125 to 0.125
- expert_down: bfloat16 [8, 3584, 2048], P('ep', 'tp')
- dense_gate: bfloat16 [2048, 5632], P('tp', 'ep'), may hold values from -0.125 to 0.125
- dense_up: bfloat16 [2048, 5632], P('tp', 'ep'), may hold values from -0.125 to 0.125
- dense_down: bfloat16 [5632, 2048], P('ep', 'tp')
- dense_mix: float32 [2048], replicated, may hold values from -0.25 to 0.25
Outputs:
- new_hidden: bfloat16 [256, 2048], P('ep', 'tp')
- new_matrix: float32 [256, 8, 128, 128], P('ep', 'tp')
- new_norm: float32 [256, 8, 128], P('ep', 'tp')
- new_max: float32 [256, 8], P('ep', 'tp')
Inputs may be any that keep to these rules, and one draw needn't show every extreme that they name: `routes`: each row names 2 different experts. Among the rows of one index of ep (an aligned block of 32 rows) no expert is named by more than 16 rows, and in every draw some expert is named by exactly 16 rows of some block.
All inputs are finite; a program needn't handle non-finite values.
Results may differ from a plain program's by a relative error of at most 0.02.
Values may be sent and summed in bfloat16 or wider, within the bound.
A program may use at most 128 MiB of HBM per device.

v0:
```python
import jax
import jax.numpy as jnp
from jax import lax
from jax.sharding import PartitionSpec as P

EPS = 1e-06


def settle(values):
    return lax.optimization_barrier(values.astype(jnp.bfloat16)).astype(jnp.float32)


def local(
    hidden,
    norm_gains,
    w_query,
    w_key,
    w_value,
    w_outgate,
    w_input_gate,
    w_forget_gate,
    forget_bias,
    w_mix_out,
    state_matrix,
    state_norm,
    state_max,
    routes,
    route_scores,
    expert_gate,
    expert_up,
    expert_down,
    dense_gate,
    dense_up,
    dense_down,
    dense_mix,
):
    tp_count = lax.axis_size("tp")
    ep_count = lax.axis_size("ep")
    tp_place = lax.axis_index("tp")
    seq_local, width = hidden.shape
    heads_local = state_matrix.shape[1]
    head_width = state_matrix.shape[2]
    part_width = width // tp_count
    feature_first = tp_place * part_width
    start_f = hidden.astype(jnp.float32)
    normed_in = (
        start_f
        * lax.rsqrt(jnp.mean(start_f * start_f, axis=-1, keepdims=True) + EPS)
        * norm_gains[0]
    ).astype(jnp.bfloat16)
    query_f = jnp.dot(normed_in, w_query, preferred_element_type=jnp.float32)
    key_f = jnp.dot(normed_in, w_key, preferred_element_type=jnp.float32)
    value_f = jnp.dot(normed_in, w_value, preferred_element_type=jnp.float32)
    gate_f = jnp.dot(normed_in, w_outgate, preferred_element_type=jnp.float32)
    head_first = tp_place * heads_local
    input_weight = lax.dynamic_slice_in_dim(w_input_gate, head_first, heads_local, 1)
    forget_weight = lax.dynamic_slice_in_dim(w_forget_gate, head_first, heads_local, 1)
    forget_local = lax.dynamic_slice_in_dim(forget_bias, head_first, heads_local, 0)
    in_gate = jnp.dot(normed_in, input_weight, preferred_element_type=jnp.float32)
    log_forget = jax.nn.log_sigmoid(
        jnp.dot(normed_in, forget_weight, preferred_element_type=jnp.float32) + forget_local
    )
    query = settle(query_f).reshape(seq_local, heads_local, head_width)
    keys = settle(key_f).reshape(seq_local, heads_local, head_width) * head_width ** (-0.5)
    values = settle(value_f).reshape(seq_local, heads_local, head_width)
    carried = log_forget + state_max
    new_max = jnp.maximum(carried, in_gate)
    keep = jnp.exp(carried - new_max)
    write = jnp.exp(in_gate - new_max)
    written = write[:, :, None] * keys
    new_matrix = (
        keep[:, :, None, None] * state_matrix + written[:, :, :, None] * values[:, :, None, :]
    )
    new_norm = keep[:, :, None] * state_norm + written
    numer = jnp.einsum("shd,shdv->shv", query, new_matrix)
    denom = jnp.einsum("shd,shd->sh", query, new_norm)
    read = numer / jnp.maximum(jnp.abs(denom), jnp.exp(-new_max))[:, :, None]
    mixed = (
        jax.nn.sigmoid(settle(gate_f)) * read.reshape(seq_local, heads_local * head_width)
    ).astype(jnp.bfloat16)
    branch_terms = settle(jnp.dot(mixed, w_mix_out, preferred_element_type=jnp.float32))
    branch = settle(
        lax.psum_scatter(
            branch_terms.astype(jnp.bfloat16), "tp", scatter_dimension=1, tiled=True
        ).astype(jnp.float32)
    )
    start_part = lax.dynamic_slice_in_dim(start_f, feature_first, part_width, 1)
    gain_rows = lax.dynamic_slice_in_dim(norm_gains, feature_first, part_width, 1)
    lifted = gain_rows[1] * branch
    mix_weight = gain_rows[2] * lax.dynamic_slice_in_dim(dense_mix, feature_first, part_width, 0)
    branch_sq, start_sq, cross_sum, lifted_sq, start_dot, lifted_dot = lax.psum(
        (
            jnp.sum(branch * branch, axis=-1),
            jnp.sum(start_part * start_part, axis=-1),
            jnp.sum(start_part * lifted, axis=-1),
            jnp.sum(lifted * lifted, axis=-1),
            jnp.sum(start_part * mix_weight, axis=-1),
            jnp.sum(lifted * mix_weight, axis=-1),
        ),
        "tp",
    )
    branch_scale = lax.rsqrt(branch_sq / width + EPS)
    residual_f = start_part + lifted * branch_scale[:, None]
    resid_sq = start_sq + 2.0 * branch_scale * cross_sum + branch_scale * branch_scale * lifted_sq
    gate_dot = start_dot + branch_scale * lifted_dot
    scale_two = lax.rsqrt(resid_sq / width + EPS)
    mix_gate = jax.nn.sigmoid(scale_two * gate_dot)
    residual = settle(residual_f)
    normed = (residual_f * scale_two[:, None] * gain_rows[2]).astype(jnp.bfloat16)
    rows_in = lax.all_gather(normed, "ep", axis=0, tiled=True)
    dense_pre = jnp.concatenate(
        [
            jnp.dot(rows_in, dense_gate, preferred_element_type=jnp.float32),
            jnp.dot(rows_in, dense_up, preferred_element_type=jnp.float32),
        ],
        axis=1,
    )
    dense_pre = lax.psum(dense_pre.astype(jnp.bfloat16), "tp").astype(jnp.float32)
    dense_pre_gate, dense_pre_up = jnp.split(dense_pre, 2, axis=1)
    dense_hidden = (jax.nn.silu(dense_pre_gate) * dense_pre_up).astype(jnp.bfloat16)
    dense_out = lax.psum_scatter(
        jnp.dot(dense_hidden, dense_down, preferred_element_type=jnp.float32).astype(jnp.bfloat16),
        "ep",
        scatter_dimension=0,
        tiled=True,
    ).astype(jnp.float32)
    route_width = routes.shape[1]
    expert_count = ep_count * expert_gate.shape[0]
    capacity = 2 * seq_local * route_width // ep_count
    flat_expert = routes.reshape(-1)
    picks = (flat_expert[:, None] == jnp.arange(expert_count, dtype=jnp.int32)[None, :]).astype(
        jnp.int32
    )
    ranks = jnp.sum(jnp.cumsum(picks, axis=0) * picks, axis=1) - 1
    slot_index = flat_expert * capacity + ranks
    placing = (
        jnp.arange(expert_count * capacity, dtype=jnp.int32)[:, None] == slot_index[None, :]
    ).astype(jnp.bfloat16)
    repeated = jnp.repeat(normed, route_width, axis=0)
    outgoing = (
        jnp.dot(placing, repeated, preferred_element_type=jnp.float32)
        .astype(jnp.bfloat16)
        .reshape(expert_count, capacity, part_width)
    )
    arrived = lax.all_to_all(outgoing, "ep", split_axis=0, concat_axis=0, tiled=True)
    full_rows = lax.all_gather(arrived, "tp", axis=2, tiled=True)
    flat_rows = full_rows.reshape(-1, width)
    gate_pre = jnp.dot(flat_rows, expert_gate[0], preferred_element_type=jnp.float32)
    up_pre = jnp.dot(flat_rows, expert_up[0], preferred_element_type=jnp.float32)
    hidden_units = (jax.nn.silu(gate_pre) * up_pre).astype(jnp.bfloat16)
    partial_out = settle(jnp.dot(hidden_units, expert_down[0], preferred_element_type=jnp.float32))
    summed_out = lax.psum_scatter(
        partial_out.astype(jnp.bfloat16), "tp", scatter_dimension=1, tiled=True
    )
    returned = lax.all_to_all(
        summed_out.reshape(arrived.shape), "ep", split_axis=0, concat_axis=0, tiled=True
    )
    picked = lax.dot_general(
        placing,
        returned.reshape(expert_count * capacity, part_width),
        (((0,), (0,)), ((), ())),
        preferred_element_type=jnp.float32,
    )
    share = route_scores / jnp.sum(route_scores, axis=-1, keepdims=True)
    moe_out = jnp.sum(
        picked.reshape(seq_local, route_width, part_width) * share[:, :, None], axis=1
    )
    ffn = moe_out + mix_gate[:, None] * dense_out
    ffn_sq = lax.psum(jnp.sum(ffn * ffn, axis=-1), "tp")
    new_hidden = (residual + gain_rows[3] * ffn * lax.rsqrt(ffn_sq / width + EPS)[:, None]).astype(
        jnp.bfloat16
    )
    return (new_hidden, new_matrix, new_norm, new_max)


def solution(mesh):
    placed = (
        P("ep", None),
        P(),
        P(None, "tp"),
        P(None, "tp"),
        P(None, "tp"),
        P(None, "tp"),
        P(),
        P(),
        P(),
        P("tp", None),
        P("ep", "tp", None, None),
        P("ep", "tp", None),
        P("ep", "tp"),
        P("ep", None),
        P("ep", None),
        P("ep", None, "tp"),
        P("ep", None, "tp"),
        P("ep", "tp", None),
        P("tp", "ep"),
        P("tp", "ep"),
        P("ep", "tp"),
        P(),
    )
    return jax.shard_map(
        local,
        mesh=mesh,
        in_specs=placed,
        out_specs=(P("ep", "tp"), P("ep", "tp", None, None), P("ep", "tp", None), P("ep", "tp")),
        check_vma=False,
    )
```

profile of v0, /device:TPU:0, one launch (start us, length us, event | category | flops | bytes accessed | tf_op | source)
XLA Modules:
  0.0 237.0 jit_solution(14512095781934341025)
XLA Ops:
  9.2 1.6 convolution_convert_fusion.7
  10.9 1.1 fusion.44
  12.8 1.2 subtract_exponential_fusion
  14.1 1.6 convolution_convert_fusion.6
  15.8 1.6 convolution_convert_fusion.5
  18.7 3.7 %multiply_add_fusion = f32[32,2,128,128]{3,2,1,0:T(8,128)S(1)} fusion(f32[32,2,128,128]{3,2,1,0:T(8,128)} %param.32, f32[32,2,128]{2,1,0:T(2,128)S(1)} %reshape.112, f32[32,2,128]{2,1,0:T(2,128)S(1)} %get-tuple-element.20, f32[32,2]{1,0:T(8,128)S(1)} %copy.31), kind=kLoop, calls=%fused_computation | loop fusion | flops 3145728 | bytes 8454400 | tf_op jit(solution)/shard_map/add | solution.py:72
  22.5 2.0 copy-done.1
  28.5 20.2 %reduce-scatter.4.cloned.1.call-done = bf16[32,512]{1,0:T(8,128)(2,1)} async-done(((bf16[32,2048]{1,0:T(8,128)(2,1)}), bf16[32,512]{1,0:T(8,128)(2,1)}) %reduce-scatter.4.cloned.1.call-update) | async-done | bytes 32784 | tf_op jit(solution)/shard_map/reduce_scatter | solution.py:83
  49.7 5.8 %all-reduce = (f32[32]{0:T(128)S(1)}, f32[32]{0:T(128)S(1)}, f32[32]{0:T(128)S(1)}, f32[32]{0:T(128)S(1)}, f32[32]{0:T(128)S(1)}, /*index=5*/f32[32]{0:T(128)S(1)}) all-reduce(f32[32]{0:T(128)S(1)} %get-tuple-element.9, f32[32]{0:T(128)S(1)} %get-tuple-element.8, f32[32]{0:T(128)S(1)} %get-tuple-element.5, ...), channel_id=1, replica_groups=mesh['ep'=8,'tp'=4] {'tp'}, use_global_device_ids=true, to_apply=%region_3.4 | all-reduce | flops 192 | bytes 1536 | tf_op jit(solution)/shard_map/psum | solution.py:91
  56.3 31.2 %all_gather.7 = bf16[256,512]{1,0:T(8,128)(2,1)S(1)} all-gather(bf16[32,512]{1,0:T(8,128)(2,1)S(1)} %get-tuple-element.23), channel_id=1, replica_groups=mesh['ep'=8,'tp'=4] {'ep'}, dimensions={0}, use_global_device_ids=true | all-gather | bytes 294912 | tf_op jit(solution)/shard_map/all_gather | solution.py:110
  89.2 5.3 %all-to-all-start = ((bf16[8,16,512]{2,1,0:T(8,128)(2,1)}), bf16[8,16,512]{2,1,0:T(8,128)(2,1)S(1)}, u32[]{:S(2)}, u32[]{:S(2)}) async-start(bf16[8,16,512]{2,1,0:T(8,128)(2,1)} %bitcast.6), calls=%async_computation.1 | async-start | bytes 262144 | tf_op jit(solution)/shard_map/all_to_all | solution.py:145
  95.5 6.3 %all-to-all-done = bf16[8,16,512]{2,1,0:T(8,128)(2,1)S(1)} async-done(((bf16[8,16,512]{2,1,0:T(8,128)(2,1)}), bf16[8,16,512]{2,1,0:T(8,128)(2,1)S(1)}, u32[]{:S(2)}, u32[]{:S(2)}) %all-to-all-start) | async-done | bytes 131104 | tf_op jit(solution)/shard_map/all_to_all | solution.py:145
  101.8 9.2 %all_gather.6 = bf16[8,16,2048]{2,1,0:T(8,128)(2,1)S(1)} all-gather(bf16[8,16,512]{2,1,0:T(8,128)(2,1)S(1)} %all-to-all-done), channel_id=1, replica_groups=mesh['ep'=8,'tp'=4] {'tp'}, dimensions={2}, use_global_device_ids=true | all-gather | bytes 655360 | tf_op jit(solution)/shard_map/all_gather | solution.py:146
  111.0 2.8 %fusion.4 = f32[128,896]{1,0:T(8,128)S(1)} fusion(bf16[128,2048]{1,0:T(8,128)(2,1)S(1)} %bitcast.51, bf16[1,2048,896]{2,1,0:T(8,128)(2,1)} %param.37), kind=kOutput, calls=%fused_computation.5 | convolution fusion | flops 469762048 | bytes 4653056 | tf_op jit(solution)/shard_map/dot_general | solution.py:148
  113.9 5.5 %fusion.6 = bf16[128,2048]{1,0:T(8,128)(2,1)} fusion(bf16[1,896,2048]{2,1,0:T(8,128)(2,1)} %param.39, bf16[128,2048]{1,0:T(8,128)(2,1)S(1)} %bitcast.52, bf16[1,2048,896]{2,1,0:T(8,128)(2,1)} %param.38, f32[128,896]{1,0:T(8,128)S(1)} %fusion.4), kind=kOutput, calls=%fused_computation.7 | convolution fusion | flops 940474368 | bytes 8847360 | tf_op jit(solution)/shard_map/dot_general | solution.py:151
  119.4 13.2 %all-reduce.3.cloned.1.call-done = bf16[256,1408]{0,1:T(8,128)(2,1)} async-done(((bf16[256,1408]{0,1:T(8,128)(2,1)}), bf16[256,1408]{0,1:T(8,128)(2,1)}) %all-reduce.3.cloned.1.call-update) | async-done | bytes 720912 | tf_op jit(solution)/shard_map/psum | solution.py:118
  132.6 1.2 convert_element_type.94
  133.8 1.1 convolution_convert_fusion.3
  134.9 21.8 %reduce-scatter.6.cloned.1.call-done = bf16[128,512]{1,0:T(8,128)(2,1)} async-done(((bf16[128,2048]{1,0:T(8,128)(2,1)}), bf16[128,512]{1,0:T(8,128)(2,1)}) %reduce-scatter.6.cloned.1.call-update) | async-done | bytes 131088 | tf_op jit(solution)/shard_map/reduce_scatter | solution.py:152
  156.7 5.5 %all-to-all-start.1 = ((bf16[8,16,512]{2,1,0:T(8,128)(2,1)}), bf16[8,16,512]{2,1,0:T(8,128)(2,1)S(1)}, u32[]{:S(2)}, u32[]{:S(2)}) async-start(bf16[8,16,512]{2,1,0:T(8,128)(2,1)} %bitcast.62), calls=%async_computation.3 | async-start | bytes 262144 | tf_op jit(solution)/shard_map/all_to_all | solution.py:155
  162.4 7.2 %all-to-all-done.1 = bf16[8,16,512]{2,1,0:T(8,128)(2,1)S(1)} async-done(((bf16[8,16,512]{2,1,0:T(8,128)(2,1)}), bf16[8,16,512]{2,1,0:T(8,128)(2,1)S(1)}, u32[]{:S(2)}, u32[]{:S(2)}) %all-to-all-start.1) | async-done | bytes 131104 | tf_op jit(solution)/shard_map/all_to_all | solution.py:155
  169.8 52.6 %reduce-scatter.8.cloned.1.call-done = bf16[32,512]{1,0:T(8,128)(2,1)} async-done(((bf16[256,512]{1,0:T(8,128)(2,1)}), bf16[32,512]{1,0:T(8,128)(2,1)}) %reduce-scatter.8.cloned.1.call-update) | async-done | bytes 32784 | tf_op jit(solution)/shard_map/reduce_scatter | solution.py:121
  223.3 5.7 %psum.63 = f32[32]{0:T(128)S(1)} all-reduce(f32[32]{0:T(128)S(1)} %multiply_reduce_fusion.1), channel_id=1, replica_groups=mesh['ep'=8,'tp'=4] {'tp'}, use_global_device_ids=true, to_apply=%region_22.23 | all-reduce | flops 32 | bytes 256 | tf_op jit(solution)/shard_map/psum | solution.py:169
  229.0 1.5 add_convert_fusion
  (73 shorter events, 14.0 us)
Async XLA Ops:
  7.2 18.1 %copy-start = (bf16[256,2048]{1,0:T(8,128)(2,1)S(1)}, bf16[256,2048]{1,0:T(8,128)(2,1)}, u32[]{:S(2)}) copy-start(bf16[256,2048]{1,0:T(8,128)(2,1)} %param.31) | copy-start | bytes 3145732
  7.2 11.2 %copy-start.2 = (bf16[32,2048]{1,0:T(8,128)(2,1)S(1)}, bf16[32,2048]{1,0:T(8,128)(2,1)}, u32[]{:S(2)}) copy-start(bf16[32,2048]{1,0:T(8,128)(2,1)} %param.22) | copy-start | bytes 393220
  7.2 10.3 %copy-start.6 = (f32[32,2,128]{2,1,0:T(2,128)S(1)}, f32[32,2,128]{2,1,0:T(2,128)}, u32[]{:S(2)}) copy-start(f32[32,2,128]{2,1,0:T(2,128)} %param.33) | copy-start | bytes 98308
  7.2 11.2 %copy-start.3 = (bf16[2048,256]{1,0:T(8,128)(2,1)S(1)}, bf16[2048,256]{1,0:T(8,128)(2,1)}, u32[]{:S(2)}) copy-start(bf16[2048,256]{1,0:T(8,128)(2,1)} %param.27) | copy-start | bytes 3145732
  7.2 41.5 %reduce-scatter.4.cloned.1.call-start = ((), (), s32[]{:S(2)}) async-start(), calls=%async_computation.5 | async-start | bytes 163840 | tf_op jit(solution)/shard_map/reduce_scatter | solution.py:83
  13.9 8.5 %copy-start.7 = (f32[32,2]{0,1:T(2,128)}, f32[32,2]{0,1:T(2,128)S(1)}, u32[]{:S(2)}) copy-start(f32[32,2]{0,1:T(2,128)S(1)} %get-tuple-element.22) | copy-start | bytes 772
  22.4 2.0 copy-start.1
  24.5 1.7 copy-start.9
  24.5 63.0 %copy-start.4 = (bf16[512,704]{0,1:T(8,128)(2,1)S(1)}, bf16[512,704]{0,1:T(8,128)(2,1)}, u32[]{:S(2)}) copy-start(bf16[512,704]{0,1:T(8,128)(2,1)} %param.41) | copy-start | bytes 2162692
  24.5 63.4 %copy-start.5 = (bf16[512,704]{0,1:T(8,128)(2,1)S(1)}, bf16[512,704]{0,1:T(8,128)(2,1)}, u32[]{:S(2)}) copy-start(bf16[512,704]{0,1:T(8,128)(2,1)} %param.40) | copy-start | bytes 2162692
  89.2 12.6 %all-to-all-start = ((bf16[8,16,512]{2,1,0:T(8,128)(2,1)}), bf16[8,16,512]{2,1,0:T(8,128)(2,1)S(1)}, u32[]{:S(2)}, u32[]{:S(2)}) async-start(bf16[8,16,512]{2,1,0:T(8,128)(2,1)} %bitcast.6), calls=%async_computation.1 | async-start | bytes 262144 | tf_op jit(solution)/shard_map/all_to_all | solution.py:145
  94.5 38.1 %all-reduce.3.cloned.1.call-start = ((), (), s32[]{:S(2)}) async-start(), calls=%async_computation.7 | async-start | bytes 1441792 | tf_op jit(solution)/shard_map/psum | solution.py:118
  95.5 61.3 %reduce-scatter.6.cloned.1.call-start = ((), (), s32[]{:S(2)}) async-start(), calls=%async_computation.6 | async-start | bytes 655360 | tf_op jit(solution)/shard_map/reduce_scatter | solution.py:152
  113.8 19.9 %copy-start.10 = (bf16[704,512]{1,0:T(8,128)(2,1)S(1)}, bf16[704,512]{1,0:T(8,128)(2,1)}, u32[]{:S(2)}) copy-start(bf16[704,512]{1,0:T(8,128)(2,1)} %param.42) | copy-start | bytes 2162692
  119.3 43.0 %copy-start.8 = (f32[32,2]{0,1:T(2,128)S(1)}, f32[32,2]{0,1:T(2,128)}, u32[]{:S(2)}) copy-start(f32[32,2]{0,1:T(2,128)} %param.36) | copy-start | bytes 772
  119.3 103.0 %reduce-scatter.8.cloned.1.call-start = ((), (), s32[]{:S(2)}) async-start(), calls=%async_computation.8 | async-start | bytes 294912 | tf_op jit(solution)/shard_map/reduce_scatter | solution.py:121
  156.7 12.9 %all-to-all-start.1 = ((bf16[8,16,512]{2,1,0:T(8,128)(2,1)}), bf16[8,16,512]{2,1,0:T(8,128)(2,1)S(1)}, u32[]{:S(2)}, u32[]{:S(2)}) async-start(bf16[8,16,512]{2,1,0:T(8,128)(2,1)} %bitcast.62), calls=%async_computation.3 | async-start | bytes 262144 | tf_op jit(solution)/shard_map/all_to_all | solution.py:155
Sparse Core Ops, SparseCore 0:
  26.3 22.3 reduce-scatter.3
  97.7 34.8 all-reduce.2
  135.0 21.6 reduce-scatter.5
  159.9 62.4 reduce-scatter.7
where the time goes:
time: 238 us; the launch traced here: 237 us
  waiting for transfers between devices  121 us (51%)
  blocking collectives  51.8 us (22%)
  matrix products  20.2 us (8%)
  between operations  14.1 us (6%)
  other arithmetic  13.3 us (6%)
  starting transfers between devices  11 us (5%)
  local copies, waits for them, and re-layouts  5.31 us (2%)
    reduce_scatter x1, waiting for transfers between devices, local(): lax.psum_scatter(jnp.dot(dense_hidden, dense_down, preferred_element_type...  52.6 us
    all_gather x1, blocking collectives, local(): rows_in = lax.all_gather(normed, 'ep', axis=0, tiled=True)  31.2 us
    reduce_scatter x1, waiting for transfers between devices, local(): lax.psum_scatter(partial_out.astype(jnp.bfloat16), 'tp', scatter_dimensio...  21.8 us
    reduce_scatter x1, waiting for transfers between devices, local(): lax.psum_scatter(branch_terms.astype(jnp.bfloat16), 'tp', scatter_dimensi...  20.2 us
    psum x1, waiting for transfers between devices, local(): lax.psum(dense_pre.astype(jnp.bfloat16), 'tp').astype(jnp.float32)  13.2 us
    all_gather x1, blocking collectives, local(): full_rows = lax.all_gather(arrived, 'tp', axis=2, tiled=True)  9.21 us
    all_to_all x1, waiting for transfers between devices, local(): lax.all_to_all(summed_out.reshape(arrived.shape), 'ep', split_axis=0, con...  7.21 us
    all_to_all x1, waiting for transfers between devices, local(): lax.all_to_all(outgoing, 'ep', split_axis=0, concat_axis=0, tiled=True)  6.31 us
  transfers between devices with their start and end apart: 6, of which 6 were waited for; matrix products, arithmetic and copies ran while one was open for 6% of the time, Pallas kernels for 0%

commit v1 on v0

v1 whole, which is shorter than its diff:
```python
import functools

import jax
import jax.numpy as jnp
from jax import lax
from jax.experimental import pallas as pl
from jax.experimental.pallas import tpu as pltpu
from jax.sharding import PartitionSpec as P

EPS = 1e-06


def settle(values):
    return lax.optimization_barrier(values.astype(jnp.bfloat16)).astype(jnp.float32)


MESH = pl.DeviceIdType.MESH


def tail_kernel(
    tp_count,
    ep_count,
    capacity,
    terms_ref,
    hidden_ref,
    gains_ref,
    mix_ref,
    codes_ref,
    combine_ref,
    share_ref,
    eg_hbm,
    eu_hbm,
    ed_hbm,
    dg_hbm,
    du_hbm,
    dd_hbm,
    out_ref,
    eg,
    eu,
    ed,
    dg,
    du,
    dd,
    br_recv,
    st_send,
    st_recv,
    fs_send,
    fs_recv,
    code_recv,
    rows_in,
    xin,
    pre_send,
    pre_recv,
    hid,
    down_send,
    down_recv,
    eo_send,
    eo_recv,
    sum_send,
    returned,
    w_sem,
    tp_send,
    tp_recv,
    ep_send,
    ep_recv,
):
    tp = lax.axis_index("tp")
    ep = lax.axis_index("ep")
    seqs, width = hidden_ref.shape
    part = width // tp_count
    rows_all = ep_count * seqs
    rows_tp = rows_all // tp_count
    first = pl.multiple_of(tp * part, part)
    f32, bf16 = jnp.float32, jnp.bfloat16

    loads = []
    for i, (src, dst) in enumerate(
        ((dg_hbm, dg), (du_hbm, du), (eg_hbm.at[0], eg), (eu_hbm.at[0], eu), (dd_hbm, dd), (ed_hbm.at[0], ed))
    ):
        load = pltpu.make_async_copy(src, dst, w_sem.at[i])
        load.start()
        loads.append(load)

    barrier = pltpu.get_barrier_semaphore()
    for d in range(1, tp_count):
        pl.semaphore_signal(
            barrier, inc=1, device_id={"tp": lax.rem(tp + d, tp_count)}, device_id_type=MESH
        )
    for d in range(1, ep_count):
        pl.semaphore_signal(
            barrier, inc=1, device_id={"ep": lax.rem(ep + d, ep_count)}, device_id_type=MESH
        )
    pl.semaphore_wait(barrier, tp_count - 1 + ep_count - 1)

    def tp_copies(phase, src_of, dst):
        made = []
        for d in range(1, tp_count):
            peer = lax.rem(tp + d, tp_count)
            copy = pltpu.make_async_remote_copy(
                src_ref=src_of(peer),
                dst_ref=dst,
                send_sem=tp_send.at[phase, d - 1],
                recv_sem=tp_recv.at[phase, d - 1],
                device_id={"tp": peer},
                device_id_type=MESH,
            )
            copy.start()
            made.append(copy)
        return made

    def ep_copies(phase, src_of, dst):
        made = []
        for d in range(1, ep_count):
            peer = lax.rem(ep + d, ep_count)
            copy = pltpu.make_async_remote_copy(
                src_ref=src_of(peer),
                dst_ref=dst,
                send_sem=ep_send.at[phase, d - 1],
                recv_sem=ep_recv.at[phase, d - 1],
                device_id={"ep": peer},
                device_id_type=MESH,
            )
            copy.start()
            made.append(copy)
        return made

    def arrive(copies):
        for copy in copies:
            copy.wait_recv()

    def left(copies):
        for copy in copies:
            copy.wait_send()

    def from_tp(d):
        return lax.rem(tp + tp_count - d, tp_count)

    def from_ep(d):
        return lax.rem(ep + ep_count - d, ep_count)

    def columns(peer):
        return pl.ds(pl.multiple_of(peer * part, part), part)

    branch_copies = tp_copies(0, lambda peer: terms_ref.at[:, columns(peer)], br_recv.at[tp])
    code_copies = ep_copies(0, lambda peer: codes_ref, code_recv.at[ep])
    start_part = hidden_ref[:, pl.ds(first, part)].astype(f32)
    gain_one = gains_ref[1:2, pl.ds(first, part)]
    gain_two = gains_ref[2:3, pl.ds(first, part)]
    gain_three = gains_ref[3:4, pl.ds(first, part)]
    mix_weight = gain_two * mix_ref[:, pl.ds(first, part)]
    start_sq = jnp.sum(start_part * start_part, axis=1, keepdims=True)
    start_dot = jnp.sum(start_part * mix_weight, axis=1, keepdims=True)
    branch = terms_ref[:, pl.ds(first, part)].astype(f32)
    arrive(branch_copies)
    for d in range(1, tp_count):
        branch = branch + br_recv[from_tp(d)].astype(f32)
    branch = branch.astype(bf16).astype(f32)
    lifted = gain_one * branch
    sums = (
        jnp.sum(branch * branch, axis=1, keepdims=True),
        start_sq,
        jnp.sum(start_part * lifted, axis=1, keepdims=True),
        jnp.sum(lifted * lifted, axis=1, keepdims=True),
        start_dot,
        jnp.sum(lifted * mix_weight, axis=1, keepdims=True),
    )
    lane = lax.broadcasted_iota(jnp.int32, (seqs, 128), 1)
    packed = jnp.zeros((seqs, 128), f32)
    for i, value in enumerate(sums):
        packed = packed + jnp.where(lane == i, value, 0.0)
    st_send[...] = packed
    stat_copies = tp_copies(1, lambda peer: st_send, st_recv.at[tp])
    arrive(stat_copies)
    for d in range(1, tp_count):
        packed = packed + st_recv[from_tp(d)]
    branch_sq, start_sq, cross_sum, lifted_sq, start_dot, lifted_dot = (
        packed[:, i : i + 1] for i in range(6)
    )
    branch_scale = lax.rsqrt(branch_sq / width + EPS)
    residual_f = start_part + lifted * branch_scale
    resid_sq = start_sq + 2.0 * branch_scale * cross_sum + branch_scale * branch_scale * lifted_sq
    gate_dot = start_dot + branch_scale * lifted_dot
    scale_two = lax.rsqrt(resid_sq / width + EPS)
    mix_gate = jax.nn.sigmoid(scale_two * gate_dot)
    residual = residual_f.astype(bf16).astype(f32)
    normed = (residual_f * scale_two * gain_two).astype(bf16)
    my_rows = pl.ds(pl.multiple_of(ep * seqs, seqs), seqs)
    rows_in[my_rows, :] = normed
    row_copies = ep_copies(1, lambda peer: rows_in.at[my_rows], rows_in.at[my_rows])

    arrive(code_copies)
    codes = codes_ref[...]
    for d in range(1, ep_count):
        codes = codes + code_recv[from_ep(d)]
    expert = lax.broadcasted_iota(jnp.int32, codes.shape, 0)
    mine = jnp.sum(jnp.where(expert == ep, codes, 0.0), axis=0, keepdims=True)
    slots = ep_count * capacity
    slot = lax.broadcasted_iota(jnp.int32, (slots, rows_all), 0)
    token = lax.broadcasted_iota(jnp.int32, (slots, rows_all), 1)
    wanted = (lax.rem(slot, capacity) + 1).astype(f32)
    placing = jnp.where(
        jnp.logical_and(slot // capacity == token // seqs, mine == wanted), 1.0, 0.0
    ).astype(bf16)

    arrive(row_copies)
    rows = rows_in[...]
    xin[tp] = jnp.dot(placing, rows, preferred_element_type=f32).astype(bf16)
    expert_copies = tp_copies(2, lambda peer: xin.at[tp], xin.at[tp])

    loads[0].wait()
    loads[1].wait()
    pre_send[0] = jnp.dot(rows, dg[...], preferred_element_type=f32).astype(bf16)
    pre_send[1] = jnp.dot(rows, du[...], preferred_element_type=f32).astype(bf16)

    def block_rows(peer):
        return pl.ds(pl.multiple_of(peer * rows_tp, rows_tp), rows_tp)

    pre_copies = tp_copies(3, lambda peer: pre_send.at[:, block_rows(peer)], pre_recv.at[tp])

    loads[2].wait()
    loads[3].wait()
    gate_pre = jnp.dot(xin[tp], eg[columns(tp), :], preferred_element_type=f32)
    up_pre = jnp.dot(xin[tp], eu[columns(tp), :], preferred_element_type=f32)
    for d in range(1, tp_count):
        expert_copies[d - 1].wait_recv()
        source = from_tp(d)
        block = xin[source]
        gate_pre = gate_pre + jnp.dot(block, eg[columns(source), :], preferred_element_type=f32)
        up_pre = up_pre + jnp.dot(block, eu[columns(source), :], preferred_element_type=f32)
    hidden_units = (jax.nn.silu(gate_pre) * up_pre).astype(bf16)

    arrive(pre_copies)
    pre = pre_send[:, block_rows(tp), :].astype(f32)
    for d in range(1, tp_count):
        pre = pre + pre_recv[from_tp(d)].astype(f32)
    hid[block_rows(tp), :] = (jax.nn.silu(pre[0]) * pre[1]).astype(bf16)
    hid_copies = tp_copies(4, lambda peer: hid.at[block_rows(tp)], hid.at[block_rows(tp)])

    loads[5].wait()
    for t in range(tp_count):
        eo_send[t] = jnp.dot(
            hidden_units, ed[:, t * part : (t + 1) * part], preferred_element_type=f32
        ).astype(bf16)
    eo_copies = tp_copies(5, lambda peer: eo_send.at[peer], eo_recv.at[tp])

    loads[4].wait()
    arrive(hid_copies)
    down_send[...] = jnp.dot(hid[...], dd[...], preferred_element_type=f32).astype(bf16)

    def seq_rows(peer):
        return pl.ds(pl.multiple_of(peer * seqs, seqs), seqs)

    down_copies = ep_copies(2, lambda peer: down_send.at[seq_rows(peer)], down_recv.at[ep])

    arrive(eo_copies)
    total = eo_send[tp].astype(f32)
    for d in range(1, tp_count):
        total = total + eo_recv[from_tp(d)].astype(f32)
    sum_send[...] = total.astype(bf16)

    def slot_rows(peer):
        return pl.ds(pl.multiple_of(peer * capacity, capacity), capacity)

    back_copies = ep_copies(3, lambda peer: sum_send.at[slot_rows(peer)], returned.at[slot_rows(ep)])
    returned[slot_rows(ep), :] = sum_send[slot_rows(ep), :]

    arrive(down_copies)
    dense_out = down_send[seq_rows(ep), :].astype(f32)
    for d in range(1, ep_count):
        dense_out = dense_out + down_recv[from_ep(d)].astype(f32)
    ffn = mix_gate * dense_out
    arrive(back_copies)
    picked = jnp.dot(combine_ref[...], returned[...], preferred_element_type=f32)
    for k in range(share_ref.shape[1]):
        ffn = ffn + share_ref[:, k : k + 1] * picked[k * seqs : (k + 1) * seqs]
    squares = jnp.where(lane == 0, jnp.sum(ffn * ffn, axis=1, keepdims=True), 0.0)
    fs_send[...] = squares
    final_copies = tp_copies(6, lambda peer: fs_send, fs_recv.at[tp])
    scaled = gain_three * ffn
    arrive(final_copies)
    for d in range(1, tp_count):
        squares = squares + fs_recv[from_tp(d)]
    out_ref[...] = (residual + scaled * lax.rsqrt(squares[:, 0:1] / width + EPS)).astype(bf16)
    for copies in (
        branch_copies,
        code_copies,
        stat_copies,
        row_copies,
        expert_copies,
        pre_copies,
        hid_copies,
        eo_copies,
        down_copies,
        back_copies,
        final_copies,
    ):
        left(copies)


def tail(
    terms, hidden, norm_gains, dense_mix, routes, route_scores, weights
):
    tp_count = lax.axis_size("tp")
    ep_count = lax.axis_size("ep")
    ep_place = lax.axis_index("ep")
    seqs, width = hidden.shape
    part = width // tp_count
    expert_gate, expert_up, expert_down, dense_gate, dense_up, dense_down = weights
    units = expert_gate.shape[2]
    dense_units = dense_gate.shape[1]
    top = routes.shape[1]
    experts = ep_count * expert_gate.shape[0]
    limit = 2 * seqs * top // ep_count
    capacity = -(-limit // 16) * 16
    rows_all = ep_count * seqs
    f32, bf16 = jnp.float32, jnp.bfloat16
    names = jnp.arange(experts, dtype=jnp.int32)
    hits = routes[:, :, None] == names[None, None, :]
    named = jnp.any(hits, axis=1)
    order = jnp.arange(seqs, dtype=jnp.int32)
    earlier = (order[None, :] < order[:, None])[:, :, None] & named[None, :, :]
    rank = jnp.sum(earlier.astype(jnp.int32), axis=1)
    code = jnp.where(named, rank + 1, 0).astype(f32)
    block = jnp.arange(ep_count, dtype=jnp.int32)[None, :, None] == ep_place
    codes = jnp.where(block, code.T[:, None, :], 0.0).reshape(experts, rows_all)
    place = jnp.arange(capacity, dtype=jnp.int32)
    combine = (
        (hits.transpose(1, 0, 2)[:, :, :, None] & (rank[None, :, :, None] == place))
        .astype(bf16)
        .reshape(top * seqs, experts * capacity)
    )
    share = route_scores / jnp.sum(route_scores, axis=-1, keepdims=True)
    vmem = pl.BlockSpec(memory_space=pltpu.VMEM)
    hbm = pl.BlockSpec(memory_space=pl.ANY)
    slots = ep_count * capacity
    return pl.pallas_call(
        functools.partial(tail_kernel, tp_count, ep_count, capacity),
        out_shape=jax.ShapeDtypeStruct((seqs, part), bf16),
        in_specs=[vmem] * 7 + [hbm] * 6,
        out_specs=vmem,
        scratch_shapes=[
            pltpu.VMEM((width, units), bf16),
            pltpu.VMEM((width, units), bf16),
            pltpu.VMEM((units, width), bf16),
            pltpu.VMEM(dense_gate.shape, bf16),
            pltpu.VMEM(dense_up.shape, bf16),
            pltpu.VMEM(dense_down.shape, bf16),
            pltpu.VMEM((tp_count, seqs, part), bf16),
            pltpu.VMEM((seqs, 128), f32),
            pltpu.VMEM((tp_count, seqs, 128), f32),
            pltpu.VMEM((seqs, 128), f32),
            pltpu.VMEM((tp_count, seqs, 128), f32),
            pltpu.VMEM((ep_count, experts, rows_all), f32),
            pltpu.VMEM((rows_all, part), bf16),
            pltpu.VMEM((tp_count, slots, part), bf16),
            pltpu.VMEM((2, rows_all, dense_units), bf16),
            pltpu.VMEM((tp_count, 2, rows_all // tp_count, dense_units), bf16),
            pltpu.VMEM((rows_all, dense_units), bf16),
            pltpu.VMEM((rows_all, part), bf16),
            pltpu.VMEM((ep_count, seqs, part), bf16),
            pltpu.VMEM((tp_count, slots, part), bf16),
            pltpu.VMEM((tp_count, slots, part), bf16),
            pltpu.VMEM((slots, part), bf16),
            pltpu.VMEM((slots, part), bf16),
            pltpu.SemaphoreType.DMA((6,)),
            pltpu.SemaphoreType.DMA((7, tp_count - 1)),
            pltpu.SemaphoreType.DMA((7, tp_count - 1)),
            pltpu.SemaphoreType.DMA((4, ep_count - 1)),
            pltpu.SemaphoreType.DMA((4, ep_count - 1)),
        ],
        compiler_params=pltpu.CompilerParams(
            collective_id=0, has_side_effects=True, vmem_limit_bytes=56 * 1024 * 1024
        ),
        name="tail",
    )(
        terms,
        hidden,
        norm_gains,
        dense_mix.reshape(1, width),
        codes,
        combine,
        share,
        *weights,
    )


def local(
    hidden,
    norm_gains,
    w_query,
    w_key,
    w_value,
    w_outgate,
    w_input_gate,
    w_forget_gate,
    forget_bias,
    w_mix_out,
    state_matrix,
    state_norm,
    state_max,
    routes,
    route_scores,
    expert_gate,
    expert_up,
    expert_down,
    dense_gate,
    dense_up,
    dense_down,
    dense_mix,
):
    tp_place = lax.axis_index("tp")
    seq_local, width = hidden.shape
    heads_local = state_matrix.shape[1]
    head_width = state_matrix.shape[2]
    start_f = hidden.astype(jnp.float32)
    normed_in = (
        start_f
        * lax.rsqrt(jnp.mean(start_f * start_f, axis=-1, keepdims=True) + EPS)
        * norm_gains[0]
    ).astype(jnp.bfloat16)
    query_f = jnp.dot(normed_in, w_query, preferred_element_type=jnp.float32)
    key_f = jnp.dot(normed_in, w_key, preferred_element_type=jnp.float32)
    value_f = jnp.dot(normed_in, w_value, preferred_element_type=jnp.float32)
    gate_f = jnp.dot(normed_in, w_outgate, preferred_element_type=jnp.float32)
    head_first = tp_place * heads_local
    input_weight = lax.dynamic_slice_in_dim(w_input_gate, head_first, heads_local, 1)
    forget_weight = lax.dynamic_slice_in_dim(w_forget_gate, head_first, heads_local, 1)
    forget_local = lax.dynamic_slice_in_dim(forget_bias, head_first, heads_local, 0)
    in_gate = jnp.dot(normed_in, input_weight, preferred_element_type=jnp.float32)
    log_forget = jax.nn.log_sigmoid(
        jnp.dot(normed_in, forget_weight, preferred_element_type=jnp.float32) + forget_local
    )
    query = settle(query_f).reshape(seq_local, heads_local, head_width)
    keys = settle(key_f).reshape(seq_local, heads_local, head_width) * head_width ** (-0.5)
    values = settle(value_f).reshape(seq_local, heads_local, head_width)
    carried = log_forget + state_max
    new_max = jnp.maximum(carried, in_gate)
    keep = jnp.exp(carried - new_max)
    write = jnp.exp(in_gate - new_max)
    written = write[:, :, None] * keys
    new_matrix = (
        keep[:, :, None, None] * state_matrix + written[:, :, :, None] * values[:, :, None, :]
    )
    new_norm = keep[:, :, None] * state_norm + written
    numer = jnp.einsum("shd,shdv->shv", query, new_matrix)
    denom = jnp.einsum("shd,shd->sh", query, new_norm)
    read = numer / jnp.maximum(jnp.abs(denom), jnp.exp(-new_max))[:, :, None]
    mixed = (
        jax.nn.sigmoid(settle(gate_f)) * read.reshape(seq_local, heads_local * head_width)
    ).astype(jnp.bfloat16)
    terms = jnp.dot(mixed, w_mix_out, preferred_element_type=jnp.float32).astype(jnp.bfloat16)
    new_hidden = tail(
        terms,
        hidden,
        norm_gains,
        dense_mix,
        routes,
        route_scores,
        (expert_gate, expert_up, expert_down, dense_gate, dense_up, dense_down),
    )
    return (new_hidden, new_matrix, new_norm, new_max)


def solution(mesh):
    placed = (
        P("ep", None),
        P(),
        P(None, "tp"),
        P(None, "tp"),
        P(None, "tp"),
        P(None, "tp"),
        P(),
        P(),
        P(),
        P("tp", None),
        P("ep", "tp", None, None),
        P("ep", "tp", None),
        P("ep", "tp"),
        P("ep", None),
        P("ep", None),
        P("ep", None, "tp"),
        P("ep", None, "tp"),
        P("ep", "tp", None),
        P("tp", "ep"),
        P("tp", "ep"),
        P("ep", "tp"),
        P(),
    )
    return jax.shard_map(
        local,
        mesh=mesh,
        in_specs=placed,
        out_specs=(P("ep", "tp"), P("ep", "tp", None, None), P("ep", "tp", None), P("ep", "tp")),
        check_vma=False,
    )
```

time: 238 us -> 84.1 us (0.35)
  waiting for transfers between devices: 121 us -> 0 us
  Pallas kernels: 0 us -> 54.3 us
  blocking collectives: 51.8 us -> 0 us
  between operations: 14.1 us -> 0.81 us
  starting transfers between devices: 11 us -> 0 us
  matrix products: 20.2 us -> 11.4 us
  other arithmetic: 13.3 us -> 9.05 us
  local copies, waits for them, and re-layouts: 5.31 us -> 8.06 us
    reduce_scatter x3 -> x0, waiting for transfers between devices: 94.7 us -> none  [the longest x1 52.6 us: local(): lax.psum_scatter(jnp.dot(dense_hidden, dense_down, preferred_element_type...]
    pallas_call x0 -> x1, Pallas kernels: none -> 54.3 us  [tail(): pl.pallas_call(functools.partial(tail_kernel, tp_count, ep_count, capacit...]
    all_gather x2 -> x0, blocking collectives: 40.4 us -> none  [the longest x1 31.2 us: local(): rows_in = lax.all_gather(normed, 'ep', axis=0, tiled=True)]
    all_to_all x2 -> x0, waiting for transfers between devices: 13.5 us -> none  [the longest x1 7.21 us: local(): lax.all_to_all(summed_out.reshape(arrived.shape), 'ep', split_axis=0, con...]
    psum x1 -> x0, waiting for transfers between devices: 13.2 us -> none  [local(): lax.psum(dense_pre.astype(jnp.bfloat16), 'tp').astype(jnp.float32)]
    psum x2 -> x0, blocking collectives: 11.4 us -> none  [the longest x1 5.77 us: local(): lax.psum((jnp.sum(branch * branch, axis=-1), jnp.sum(start_part * start_p...]
    dot_general x7 -> x0, matrix products: 11.1 us -> none  [the longest x1 5.45 us: local(): jnp.dot(hidden_units, expert_down[0], preferred_element_type=jnp.float32)]
    all_to_all x2 -> x0, starting transfers between devices: 10.8 us -> none  [the longest x1 5.52 us: local(): lax.all_to_all(summed_out.reshape(arrived.shape), 'ep', split_axis=0, con...]
  transfers between devices with their start and end apart: 6 -> 0, of which waited for: 6 -> 0; matrix products, arithmetic and copies ran while one was open for 6% -> 0% of each run, Pallas kernels for 0% -> 0%
where the time goes in v1:
time: 84.1 us; the launch traced here: 83.6 us
  Pallas kernels  54.3 us (65%)
  matrix products  11.4 us (14%)
  other arithmetic  9.05 us (11%)
  local copies, waits for them, and re-layouts  8.06 us (10%)
    pallas_call x1, Pallas kernels, tail(): pl.pallas_call(functools.partial(tail_kernel, tp_count, ep_count, capacit...  54.3 us
    unnamed x18, local copies, waits for them, and re-layouts  4.94 us
    add x1, other arithmetic, local(): keep[:, :, None, None] * state_matrix  4.32 us
    dot_general x1, matrix products, local(): numer = jnp.einsum('shd,shdv->shv', query, new_matrix)  2.97 us

profile of v1, /device:TPU:0, one launch (start us, length us, event | category | flops | bytes accessed | tf_op | source)
XLA Modules:
  0.0 83.6 jit_solution(183189562713254393)
XLA Ops:
  0.7 0.9 %slice.3 = f32[1,2048]{1,0:T(1,128)S(1)} slice(f32[4,2048]{1,0:T(4,128)} %gains_ref.1), slice={[0:1], [0:2048]} | slice | bytes 16384 | tf_op jit(solution)/shard_map/slice | solution.py:419
  1.5 1.0 %fusion.1 = f32[32]{0:T(128)S(1)} fusion(bf16[32,2048]{1,0:T(8,128)(2,1)} %hidden_ref.1), kind=kLoop, calls=%fused_computation.10 | loop fusion | flops 196576 | bytes 131200 | tf_op jit(solution)/shard_map/reduce_sum | solution.py:418
  2.5 1.1 %fusion.8 = f32[32,2]{0,1:T(2,128)S(1)} fusion(bf16[2048,8]{0,1:T(8,128)(2,1)} %param.28, s32[]{:T(128)S(6)} %select_n.21, bf16[32,2048]{1,0:T(8,128)(2,1)} %hidden_ref.1, f32[2048]{0:T(1024)S(1)} %bitcast.22, f32[32]{0:T(128)S(1)} %add_rsqrt_fusion), kind=kOutput, calls=%fused_computation.28 | convolution fusion | flops 524288 | bytes 147844 | tf_op jit(solution)/shard_map/dot_general | solution.py:429
  3.7 0.7 dynamic_slice.10
  4.4 1.2 %subtract_exponential_fusion = (f32[32,2]{0,1:T(2,128)S(1)}, f32[32,2]{0,1:T(2,128)S(1)}) fusion(f32[32,2]{0,1:T(2,128)S(1)} %fusion.8, f32[32,2]{0,1:T(2,128)} %param.34, f32[2]{0:T(128)S(1)} %dynamic_slice.10, bf16[2048,8]{0,1:T(8,128)(2,1)} %param.29, s32[]{:T(128)S(6)} %select_n.21, bf16[32,2048]{1,0:T(8,128)(2,1)} %hidden_ref.1, ...), kind=kOutput, calls=%fused_computation.39 | convolution fusion | flops 525056 | bytes 149388 | tf_op jit(solution)/shard_map/dot_general | solution.py:431
  5.8 1.6 %convolution_convert_fusion.3 = bf16[32,256]{1,0:T(8,128)(2,1)S(1)} fusion(bf16[2048,256]{1,0:T(8,128)(2,1)} %param.24, bf16[32,2048]{1,0:T(8,128)(2,1)} %hidden_ref.1, f32[2048]{0:T(1024)S(1)} %bitcast.24, f32[32]{0:T(128)S(1)} %add_rsqrt_fusion), kind=kOutput, calls=%fused_computation.4 | convolution fusion | flops 33824768 | bytes 1204352 | tf_op jit(solution)/shard_map/dot_general | solution.py:421
  7.4 1.6 %convolution_convert_fusion.2 = bf16[32,256]{1,0:T(8,128)(2,1)S(1)} fusion(bf16[2048,256]{1,0:T(8,128)(2,1)} %param.25, bf16[32,2048]{1,0:T(8,128)(2,1)} %hidden_ref.1, f32[2048]{0:T(1024)S(1)} %bitcast.25, f32[32]{0:T(128)S(1)} %add_rsqrt_fusion), kind=kOutput, calls=%fused_computation.3 | convolution fusion | flops 33824768 | bytes 1204352 | tf_op jit(solution)/shard_map/dot_general | solution.py:422
  9.1 1.5 %fusion.5 = (f32[32,2]{1,0:T(8,128)S(1)}, f32[32,2,128]{2,1,0:T(2,128)}, f32[32,2,128]{2,1,0:T(2,128)S(1)}) fusion(bf16[32,2,128]{2,1,0:T(2,128)(2,1)S(1)} %reshape.85, f32[32,2,128]{2,1,0:T(2,128)} %param.33, f32[32,2]{1,0:T(8,128)S(1)} %copy.56, f32[32,2,128]{2,1,0:T(2,128)S(1)} %reshape.91, f32[32,2]{1,0:T(8,128)S(1)} %copy.57), kind=kLoop, calls=%fused_computation.19 | loop fusion | flops 49088 | bytes 148224
  10.6 1.6 %convolution_convert_fusion.1 = bf16[32,256]{1,0:T(8,128)(2,1)S(1)} fusion(bf16[2048,256]{1,0:T(8,128)(2,1)} %param.26, bf16[32,2048]{1,0:T(8,128)(2,1)} %hidden_ref.1, f32[2048]{0:T(1024)S(1)} %bitcast.26, f32[32]{0:T(128)S(1)} %add_rsqrt_fusion), kind=kOutput, calls=%fused_computation.2 | convolution fusion | flops 33824768 | bytes 1204352 | tf_op jit(solution)/shard_map/dot_general | solution.py:423
  12.3 4.3 %multiply_add_fusion = f32[32,2,128,128]{3,2,1,0:T(8,128)} fusion(f32[32,2,128,128]{3,2,1,0:T(8,128)} %param.32, f32[32,2,128]{2,1,0:T(2,128)S(1)} %reshape.92, f32[32,2,128]{2,1,0:T(2,128)S(1)} %get-tuple-element.6, f32[32,2]{1,0:T(8,128)S(1)} %copy.56), kind=kLoop, calls=%fused_computation | loop fusion | flops 3145728 | bytes 8454400 | tf_op jit(solution)/shard_map/add | solution.py:442
  16.6 3.0 %fusion.25 = f32[32,2,1,128]{3,2,1,0:T(1,128)S(1)} fusion(bf16[32,2,128,1]{2,3,1,0:T(2,128)(2,1)S(1)} %reshape.99, f32[32,2,128,128]{3,2,1,0:T(8,128)} %multiply_add_fusion), kind=kOutput, calls=%fused_computation.45 | convolution fusion | flops 2097152 | bytes 4243456 | tf_op jit(solution)/shard_map/shd,shdv->shv/dot_general | solution.py:445
  19.8 0.1 broadcast_divide_fusion
  19.9 0.3 convolution_convert_fusion.4
  20.3 0.9 %convolution_convert_fusion.terms_ref = bf16[32,2048]{1,0:T(8,128)(2,1)} fusion(bf16[256,2048]{1,0:T(8,128)(2,1)S(1)} %copy-done, f32[4,8,2,128]{3,2,1,0:T(2,128)S(1)} %bitcast.29, bf16[32,256]{1,0:T(8,128)(2,1)S(1)} %convolution_convert_fusion.4), kind=kOutput, calls=%fused_computation.1 | convolution fusion | flops 33669120 | bytes 1228800 | tf_op jit(solution)/shard_map/dot_general | solution.py:451
  21.2 0.6 convert_reduce_fusion
  22.1 0.1 broadcast_in_dim.31
  22.2 0.6 broadcast_select_fusion.codes_ref
  22.9 0.1 reshape.93
  23.0 0.7 copy.64.combine_ref
  23.7 1.2 %copy.65.dg_hbm = bf16[512,704]{1,0:T(8,128)(2,1)} copy(bf16[512,704]{0,1:T(8,128)(2,1)S(1)} %copy-done.3) | data formatting | bytes 1441792 | tf_op args[18]
  24.8 2.3 %copy.66.du_hbm = bf16[512,704]{1,0:T(8,128)(2,1)} copy(bf16[512,704]{0,1:T(8,128)(2,1)} %param.41) | data formatting | bytes 1441792 | tf_op args[19]
  27.2 0.7 broadcast_divide_fusion.1.share_ref
  27.9 54.3 %tail.1 = bf16[32,512]{1,0:T(8,128)(2,1)} custom-call(bf16[32,2048]{1,0:T(8,128)(2,1)} %convolution_convert_fusion.terms_ref, bf16[32,2048]{1,0:T(8,128)(2,1)} %hidden_ref.1, f32[4,2048]{1,0:T(4,128)} %gains_ref.1, f32[1,2048]{1,0:T(1,128)} %bitcast.30, f32[8,256]{1,0:T(8,128)} %broadcast_select_fusion.codes_ref, bf16[64,128]{1,0:T(8,128)(2,1)} %copy.64.combine_ref, ...), custom_call_target="tpu_custom_call" | custom-call | tf_op jit(solution)/shard_map/tail/pallas_call | solution.py:336
  82.2 1.4 %copy.78 = bf16[32,512]{1,0:T(8,128)(2,1)} copy(bf16[32,512]{1,0:T(8,128)(2,1)} %tail.1) | data formatting | bytes 65536
  (38 shorter events, 1.0 us)
Async XLA Ops:
  0.6 19.6 %copy-start = (bf16[256,2048]{1,0:T(8,128)(2,1)S(1)}, bf16[256,2048]{1,0:T(8,128)(2,1)}, u32[]{:S(2)}) copy-start(bf16[256,2048]{1,0:T(8,128)(2,1)} %param.31) | copy-start | bytes 3145732
  5.6 14.1 %copy-start.4 = (f32[32,2]{0,1:T(2,128)}, f32[32,2]{0,1:T(2,128)S(1)}, u32[]{:S(2)}) copy-start(f32[32,2]{0,1:T(2,128)S(1)} %get-tuple-element.16) | copy-start | bytes 772
  16.6 3.3 %copy-start.1 = (bf16[32,2048]{1,0:T(8,128)(2,1)S(1)}, bf16[32,2048]{1,0:T(8,128)(2,1)}, u32[]{:S(2)}) copy-start(bf16[32,2048]{1,0:T(8,128)(2,1)} %hidden_ref.1) | copy-start | bytes 393220
  16.6 3.3 %copy-start.2 = (bf16[2048,256]{1,0:T(8,128)(2,1)S(1)}, bf16[2048,256]{1,0:T(8,128)(2,1)}, u32[]{:S(2)}) copy-start(bf16[2048,256]{1,0:T(8,128)(2,1)} %param.27) | copy-start | bytes 3145732
  16.6 4.6 %copy-start.5 = (s32[32,2]{0,1:T(2,128)S(1)}, s32[32,2]{0,1:T(2,128)}, u32[]{:S(2)}) copy-start(s32[32,2]{0,1:T(2,128)} %param.35) | copy-start | bytes 772
  16.6 7.1 %copy-start.3 = (bf16[512,704]{0,1:T(8,128)(2,1)S(1)}, bf16[512,704]{0,1:T(8,128)(2,1)}, u32[]{:S(2)}) copy-start(bf16[512,704]{0,1:T(8,128)(2,1)} %param.40) | copy-start | bytes 2162692
  16.6 10.5 %copy-start.6 = (f32[32,2]{0,1:T(2,128)S(1)}, f32[32,2]{0,1:T(2,128)}, u32[]{:S(2)}) copy-start(f32[32,2]{0,1:T(2,128)} %param.36) | copy-start | bytes 772

commit v2 on v1

--- a/solution.py
+++ b/solution.py
@@ -10,8 +10,168 @@
 EPS = 1e-06
 
 
-def settle(values):
-    return lax.optimization_barrier(values.astype(jnp.bfloat16)).astype(jnp.float32)
+def front_kernel(
+    hidden_ref,
+    gains_ref,
+    in_ref,
+    forget_ref,
+    bias_ref,
+    norm_ref,
+    max_ref,
+    wq_hbm,
+    wk_hbm,
+    wv_hbm,
+    wo_hbm,
+    wm_hbm,
+    state_hbm,
+    terms_ref,
+    matrix_hbm,
+    new_norm_ref,
+    new_max_ref,
+    wq,
+    wk,
+    wv,
+    wo,
+    wm,
+    state,
+    numer,
+    w_sem,
+    in_sem,
+    out_sem,
+):
+    tp = lax.axis_index("tp")
+    f32, bf16 = jnp.float32, jnp.bfloat16
+    seqs = hidden_ref.shape[0]
+    heads, head = state.shape[1], state.shape[2]
+    chunks = in_sem.shape[0]
+    step = seqs // chunks
+    loads = []
+    for i, (src, dst) in enumerate(((wk_hbm, wk), (wq_hbm, wq), (wv_hbm, wv), (wo_hbm, wo))):
+        loads.append(pltpu.make_async_copy(src, dst, w_sem.at[i]))
+        loads[i].start()
+    fetches = []
+    for c in range(chunks):
+        rows = pl.ds(c * step, step)
+        fetches.append(pltpu.make_async_copy(state_hbm.at[rows], state.at[rows], in_sem.at[c]))
+        fetches[c].start()
+    loads.append(pltpu.make_async_copy(wm_hbm, wm, w_sem.at[4]))
+    loads[4].start()
+
+    start = hidden_ref[...].astype(f32)
+    scale = lax.rsqrt(jnp.mean(start * start, axis=1, keepdims=True) + EPS)
+    normed = (start * scale * gains_ref[0:1, :]).astype(bf16)
+    last = (((1,), (1,)), ((), ()))
+    in_all = lax.dot_general(normed, in_ref[...], last, preferred_element_type=f32)
+    forget_all = lax.dot_general(normed, forget_ref[...], last, preferred_element_type=f32)
+    forget_all = forget_all + bias_ref[...]
+    forget_all = jnp.minimum(forget_all, 0.0) - jnp.log(1.0 + jnp.exp(-jnp.abs(forget_all)))
+    column = lax.broadcasted_iota(jnp.int32, in_all.shape, 1)
+    here = lax.broadcasted_iota(jnp.int32, (seqs, seqs), 0)
+    there = lax.broadcasted_iota(jnp.int32, (seqs, seqs), 1)
+    projected = []
+    for i, weight in enumerate((wk, wq, wv)):
+        loads[i].wait()
+        product = jnp.dot(normed, weight[...], preferred_element_type=f32)
+        projected.append(product.astype(bf16).astype(f32))
+    keys, query, values = projected
+    pieces = []
+    for h in range(heads):
+        span = slice(h * head, (h + 1) * head)
+        pieces.extend((keys[:, span], query[:, span]))
+    turned = jnp.concatenate(pieces, axis=0).T
+    keeps = []
+    adds = []
+    bounds = []
+    for h in range(heads):
+        span = slice(h * head, (h + 1) * head)
+        mine = column == tp * heads + h
+        in_gate = jnp.sum(jnp.where(mine, in_all, 0.0), axis=1, keepdims=True)
+        log_forget = jnp.sum(jnp.where(mine, forget_all, 0.0), axis=1, keepdims=True)
+        before = jnp.sum(jnp.where(here == there, max_ref[h : h + 1, :], 0.0), axis=1, keepdims=True)
+        carried = log_forget + before
+        new_max = jnp.maximum(carried, in_gate)
+        keep = jnp.exp(carried - new_max)
+        write = jnp.exp(in_gate - new_max) * head ** (-0.5)
+        new_max_ref[h : h + 1, :] = jnp.sum(
+            jnp.where(here == there, new_max, 0.0), axis=0, keepdims=True
+        )
+        new_norm = keep * norm_ref[:, h, :] + write * keys[:, span]
+        new_norm_ref[:, h, :] = new_norm
+        denom = jnp.sum(query[:, span] * new_norm, axis=1, keepdims=True)
+        bounds.append(jnp.maximum(jnp.abs(denom), jnp.exp(-new_max)))
+        keeps.append(jnp.broadcast_to(keep, (seqs, head)))
+        adds.append(write * values[:, span])
+    stores = []
+    for c in range(chunks):
+        fetches[c].wait()
+        for s in range(c * step, (c + 1) * step):
+            for h in range(heads):
+                at = 2 * h * seqs + s
+                key_col = turned[:, at : at + 1]
+                query_col = turned[:, at + seqs : at + seqs + 1]
+                new = keeps[h][s : s + 1, :] * state[s, h] + key_col * adds[h][s : s + 1, :]
+                state[s, h] = new
+                numer[h, s : s + 1, :] = jnp.sum(query_col * new, axis=0, keepdims=True)
+        rows = pl.ds(c * step, step)
+        stores.append(pltpu.make_async_copy(state.at[rows], matrix_hbm.at[rows], out_sem.at[c]))
+        stores[c].start()
+    loads[3].wait()
+    gate = jnp.dot(normed, wo[...], preferred_element_type=f32).astype(bf16).astype(f32)
+    mixed = []
+    for h in range(heads):
+        span = slice(h * head, (h + 1) * head)
+        mixed.append((jax.nn.sigmoid(gate[:, span]) * (numer[h] / bounds[h])).astype(bf16))
+    mixed = jnp.concatenate(mixed, axis=1)
+    loads[4].wait()
+    part = terms_ref.shape[2]
+    for t in range(terms_ref.shape[0]):
+        terms_ref[t] = jnp.dot(
+            mixed, wm[:, t * part : (t + 1) * part], preferred_element_type=f32
+        ).astype(bf16)
+    for store in stores:
+        store.wait()
+
+
+def front(hidden, norm_gains, gate_weights, forget_bias, state_norm, state_max, weights, state_matrix):
+    tp_count = lax.axis_size("tp")
+    seqs, width = hidden.shape
+    heads, head = state_matrix.shape[1], state_matrix.shape[2]
+    f32, bf16 = jnp.float32, jnp.bfloat16
+    chunks = 4
+    vmem = pl.BlockSpec(memory_space=pltpu.VMEM)
+    hbm = pl.BlockSpec(memory_space=pl.ANY)
+    terms, matrix, norm, top = pl.pallas_call(
+        front_kernel,
+        out_shape=(
+            jax.ShapeDtypeStruct((tp_count, seqs, width // tp_count), bf16),
+            jax.ShapeDtypeStruct(state_matrix.shape, f32),
+            jax.ShapeDtypeStruct(state_norm.shape, f32),
+            jax.ShapeDtypeStruct((heads, seqs), f32),
+        ),
+        in_specs=[vmem] * 7 + [hbm] * 6,
+        out_specs=(vmem, hbm, vmem, vmem),
+        scratch_shapes=[pltpu.VMEM(weight.shape, bf16) for weight in weights]
+        + [
+            pltpu.VMEM(state_matrix.shape, f32),
+            pltpu.VMEM((heads, seqs, head), f32),
+            pltpu.SemaphoreType.DMA((5,)),
+            pltpu.SemaphoreType.DMA((chunks,)),
+            pltpu.SemaphoreType.DMA((chunks,)),
+        ],
+        compiler_params=pltpu.CompilerParams(vmem_limit_bytes=40 * 1024 * 1024),
+        name="front",
+    )(
+        hidden,
+        norm_gains,
+        gate_weights[0].T,
+        gate_weights[1].T,
+        forget_bias.reshape(1, -1),
+        state_norm,
+        state_max.T,
+        *weights,
+        state_matrix,
+    )
+    return terms, matrix, norm, top.T
 
 
 MESH = pl.DeviceIdType.MESH
@@ -25,9 +185,8 @@
     hidden_ref,
     gains_ref,
     mix_ref,
-    codes_ref,
-    combine_ref,
-    share_ref,
+    routes_ref,
+    scores_ref,
     eg_hbm,
     eu_hbm,
     ed_hbm,
@@ -46,16 +205,21 @@
     st_recv,
     fs_send,
     fs_recv,
+    code_send,
     code_recv,
     rows_in,
     xin,
     pre_send,
-    pre_recv,
+    pre_one,
+    pre_mid,
+    pre_two,
     hid,
     down_send,
     down_recv,
     eo_send,
-    eo_recv,
+    eo_one,
+    eo_mid,
+    eo_two,
     sum_send,
     returned,
     w_sem,
@@ -108,6 +272,58 @@
             made.append(copy)
         return made
 
+    groups = tp_count // 2
+    parity = lax.rem(tp, 2)
+    group = tp // 2
+    pair = tp + 1 - 2 * parity
+
+    def one_copy(phase, i, src, dst, peer):
+        copy = pltpu.make_async_remote_copy(
+            src_ref=src,
+            dst_ref=dst,
+            send_sem=tp_send.at[phase, i],
+            recv_sem=tp_recv.at[phase, i],
+            device_id={"tp": peer},
+            device_id_type=MESH,
+        )
+        copy.start()
+        return copy
+
+    def ahead(d):
+        return lax.rem(group + d, groups) * 2 + parity
+
+    def behind(d):
+        return lax.rem(group + groups - d, groups) * 2 + parity
+
+    def gather_start(phase, at):
+        made = [one_copy(phase, d - 1, at(tp), at(tp), ahead(d)) for d in range(1, groups)]
+        made.append(one_copy(phase, groups - 1, at(tp), at(tp), pair))
+        return made
+
+    def gather_relay(phase, at, made):
+        for d in range(1, groups):
+            made[d - 1].wait_recv()
+            made.append(one_copy(phase, groups - 1 + d, at(behind(d)), at(behind(d)), pair))
+
+    def scatter_pair(phase, at, one):
+        return [
+            one_copy(phase, j, at(j * 2 + 1 - parity), one.at[j], pair) for j in range(groups)
+        ]
+
+    def scatter_cross(phase, at, one, mid, two, made):
+        arrive(made)
+        for d in range(1, groups):
+            j = lax.rem(group + d, groups)
+            mid[j] = (at(ahead(d))[...].astype(f32) + one[j].astype(f32)).astype(bf16)
+            made.append(one_copy(phase, groups + d - 1, mid.at[j], two.at[group], ahead(d)))
+
+    def scatter_sum(at, one, two, made):
+        total = at(tp)[...].astype(f32) + one[group].astype(f32)
+        for d in range(1, groups):
+            made[groups + d - 1].wait_recv()
+            total = total + two[lax.rem(group + groups - d, groups)].astype(f32)
+        return total
+
     def ep_copies(phase, src_of, dst):
         made = []
         for d in range(1, ep_count):
@@ -141,8 +357,42 @@
     def columns(peer):
         return pl.ds(pl.multiple_of(peer * part, part), part)
 
-    branch_copies = tp_copies(0, lambda peer: terms_ref.at[:, columns(peer)], br_recv.at[tp])
-    code_copies = ep_copies(0, lambda peer: codes_ref, code_recv.at[ep])
+    branch_copies = tp_copies(0, lambda peer: terms_ref.at[peer], br_recv.at[tp])
+    top = routes_ref.shape[0]
+    experts = code_send.shape[0]
+    name = lax.broadcasted_iota(jnp.int32, (experts, seqs), 0)
+    hits = [routes_ref[k : k + 1, :] == name for k in range(top)]
+    named = hits[0]
+    for k in range(1, top):
+        named = jnp.logical_or(named, hits[k])
+    named = jnp.where(named, 1.0, 0.0)
+    here = lax.broadcasted_iota(jnp.int32, (seqs, seqs), 0)
+    there = lax.broadcasted_iota(jnp.int32, (seqs, seqs), 1)
+    before = jnp.where(here < there, 1.0, 0.0).astype(bf16)
+    rank = jnp.dot(named.astype(bf16), before, preferred_element_type=f32) + 1.0
+    code = (named * rank).astype(bf16)
+    from_row = lax.broadcasted_iota(jnp.int32, (seqs, rows_all), 0)
+    to_row = lax.broadcasted_iota(jnp.int32, (seqs, rows_all), 1)
+    spread = jnp.where(from_row + ep * seqs == to_row, 1.0, 0.0).astype(bf16)
+    code_send[...] = jnp.dot(code, spread, preferred_element_type=f32)
+    code_copies = ep_copies(0, lambda peer: code_send, code_recv.at[ep])
+    slots = ep_count * capacity
+    owner = lax.broadcasted_iota(jnp.int32, (slots, experts), 0) // capacity
+    of_expert = lax.broadcasted_iota(jnp.int32, (slots, experts), 1)
+    widen = jnp.where(owner == of_expert, 1.0, 0.0).astype(bf16)
+    row_slot = lax.broadcasted_iota(jnp.int32, (slots, seqs), 0)
+    row_wanted = (lax.rem(row_slot, capacity) + 1).astype(f32)
+    combines = []
+    shares = []
+    score_sum = scores_ref[0:1, :]
+    for k in range(1, top):
+        score_sum = score_sum + scores_ref[k : k + 1, :]
+    for k in range(top):
+        code_k = jnp.where(hits[k], rank, 0.0).astype(bf16)
+        wide = jnp.dot(widen, code_k, preferred_element_type=f32)
+        combines.append(jnp.where(wide == row_wanted, 1.0, 0.0).astype(bf16))
+        share = scores_ref[k : k + 1, :] / score_sum
+        shares.append(jnp.sum(jnp.where(here == there, share, 0.0), axis=1, keepdims=True))
     start_part = hidden_ref[:, pl.ds(first, part)].astype(f32)
     gain_one = gains_ref[1:2, pl.ds(first, part)]
     gain_two = gains_ref[2:3, pl.ds(first, part)]
@@ -150,7 +400,7 @@
     mix_weight = gain_two * mix_ref[:, pl.ds(first, part)]
     start_sq = jnp.sum(start_part * start_part, axis=1, keepdims=True)
     start_dot = jnp.sum(start_part * mix_weight, axis=1, keepdims=True)
-    branch = terms_ref[:, pl.ds(first, part)].astype(f32)
+    branch = terms_ref[tp].astype(f32)
     arrive(branch_copies)
     for d in range(1, tp_count):
         branch = branch + br_recv[from_tp(d)].astype(f32)
@@ -189,12 +439,11 @@
     row_copies = ep_copies(1, lambda peer: rows_in.at[my_rows], rows_in.at[my_rows])
 
     arrive(code_copies)
-    codes = codes_ref[...]
+    codes = code_send[...]
     for d in range(1, ep_count):
         codes = codes + code_recv[from_ep(d)]
     expert = lax.broadcasted_iota(jnp.int32, codes.shape, 0)
     mine = jnp.sum(jnp.where(expert == ep, codes, 0.0), axis=0, keepdims=True)
-    slots = ep_count * capacity
     slot = lax.broadcasted_iota(jnp.int32, (slots, rows_all), 0)
     token = lax.broadcasted_iota(jnp.int32, (slots, rows_all), 1)
     wanted = (lax.rem(slot, capacity) + 1).astype(f32)
@@ -205,46 +454,67 @@
     arrive(row_copies)
     rows = rows_in[...]
     xin[tp] = jnp.dot(placing, rows, preferred_element_type=f32).astype(bf16)
-    expert_copies = tp_copies(2, lambda peer: xin.at[tp], xin.at[tp])
+    def block_rows(peer):
+        return pl.ds(pl.multiple_of(peer * rows_tp, rows_tp), rows_tp)
+
+    def xin_at(i):
+        return xin.at[i]
+
+    def pre_at(i):
+        return pre_send.at[:, block_rows(i)]
+
+    def hid_at(i):
+        return hid.at[block_rows(i)]
+
+    def eo_at(i):
+        return eo_send.at[i]
+
+    expert_copies = gather_start(2, xin_at)
 
     loads[0].wait()
     loads[1].wait()
-    pre_send[0] = jnp.dot(rows, dg[...], preferred_element_type=f32).astype(bf16)
-    pre_send[1] = jnp.dot(rows, du[...], preferred_element_type=f32).astype(bf16)
-
-    def block_rows(peer):
-        return pl.ds(pl.multiple_of(peer * rows_tp, rows_tp), rows_tp)
-
-    pre_copies = tp_copies(3, lambda peer: pre_send.at[:, block_rows(peer)], pre_recv.at[tp])
+    last = (((1,), (1,)), ((), ()))
+    pre_send[0] = lax.dot_general(rows, dg[...], last, preferred_element_type=f32).astype(bf16)
+    pre_send[1] = lax.dot_general(rows, du[...], last, preferred_element_type=f32).astype(bf16)
+    pre_copies = scatter_pair(3, pre_at, pre_one)
 
     loads[2].wait()
     loads[3].wait()
     gate_pre = jnp.dot(xin[tp], eg[columns(tp), :], preferred_element_type=f32)
     up_pre = jnp.dot(xin[tp], eu[columns(tp), :], preferred_element_type=f32)
-    for d in range(1, tp_count):
-        expert_copies[d - 1].wait_recv()
-        source = from_tp(d)
-        block = xin[source]
-        gate_pre = gate_pre + jnp.dot(block, eg[columns(source), :], preferred_element_type=f32)
-        up_pre = up_pre + jnp.dot(block, eu[columns(source), :], preferred_element_type=f32)
+    scatter_cross(3, pre_at, pre_one, pre_mid, pre_two, pre_copies)
+    expert_copies[groups - 1].wait_recv()
+    gate_pre = gate_pre + jnp.dot(xin[pair], eg[columns(pair), :], preferred_element_type=f32)
+    up_pre = up_pre + jnp.dot(xin[pair], eu[columns(pair), :], preferred_element_type=f32)
+    gather_relay(2, xin_at, expert_copies)
+    for d in range(1, groups):
+        source = behind(d)
+        gate_pre = gate_pre + jnp.dot(xin[source], eg[columns(source), :], preferred_element_type=f32)
+        up_pre = up_pre + jnp.dot(xin[source], eu[columns(source), :], preferred_element_type=f32)
+    for d in range(1, groups):
+        expert_copies[groups - 1 + d].wait_recv()
+        source = behind(d) + 1 - 2 * parity
+        gate_pre = gate_pre + jnp.dot(xin[source], eg[columns(source), :], preferred_element_type=f32)
+        up_pre = up_pre + jnp.dot(xin[source], eu[columns(source), :], preferred_element_type=f32)
     hidden_units = (jax.nn.silu(gate_pre) * up_pre).astype(bf16)
 
-    arrive(pre_copies)
-    pre = pre_send[:, block_rows(tp), :].astype(f32)
-    for d in range(1, tp_count):
-        pre = pre + pre_recv[from_tp(d)].astype(f32)
+    pre = scatter_sum(pre_at, pre_one, pre_two, pre_copies)
     hid[block_rows(tp), :] = (jax.nn.silu(pre[0]) * pre[1]).astype(bf16)
-    hid_copies = tp_copies(4, lambda peer: hid.at[block_rows(tp)], hid.at[block_rows(tp)])
+    hid_copies = gather_start(4, hid_at)
 
     loads[5].wait()
-    for t in range(tp_count):
-        eo_send[t] = jnp.dot(
-            hidden_units, ed[:, t * part : (t + 1) * part], preferred_element_type=f32
-        ).astype(bf16)
-    eo_copies = tp_copies(5, lambda peer: eo_send.at[peer], eo_recv.at[tp])
-
+    for j in range(groups):
+        t = j * 2 + 1 - parity
+        eo_send[t] = jnp.dot(hidden_units, ed[:, columns(t)], preferred_element_type=f32).astype(bf16)
+    eo_copies = scatter_pair(5, eo_at, eo_one)
+    for j in range(groups):
+        t = j * 2 + parity
+        eo_send[t] = jnp.dot(hidden_units, ed[:, columns(t)], preferred_element_type=f32).astype(bf16)
+    scatter_cross(5, eo_at, eo_one, eo_mid, eo_two, eo_copies)
+    gather_relay(4, hid_at, hid_copies)
+    for copy in hid_copies[groups - 1 :]:
+        copy.wait_recv()
     loads[4].wait()
-    arrive(hid_copies)
     down_send[...] = jnp.dot(hid[...], dd[...], preferred_element_type=f32).astype(bf16)
 
     def seq_rows(peer):
@@ -252,10 +522,7 @@
 
     down_copies = ep_copies(2, lambda peer: down_send.at[seq_rows(peer)], down_recv.at[ep])
 
-    arrive(eo_copies)
-    total = eo_send[tp].astype(f32)
-    for d in range(1, tp_count):
-        total = total + eo_recv[from_tp(d)].astype(f32)
+    total = scatter_sum(eo_at, eo_one, eo_two, eo_copies)
     sum_send[...] = total.astype(bf16)
 
     def slot_rows(peer):
@@ -270,9 +537,10 @@
         dense_out = dense_out + down_recv[from_ep(d)].astype(f32)
     ffn = mix_gate * dense_out
     arrive(back_copies)
-    picked = jnp.dot(combine_ref[...], returned[...], preferred_element_type=f32)
-    for k in range(share_ref.shape[1]):
-        ffn = ffn + share_ref[:, k : k + 1] * picked[k * seqs : (k + 1) * seqs]
+    first_dims = (((0,), (0,)), ((), ()))
+    for k in range(top):
+        picked = lax.dot_general(combines[k], returned[...], first_dims, preferred_element_type=f32)
+        ffn = ffn + shares[k] * picked
     squares = jnp.where(lane == 0, jnp.sum(ffn * ffn, axis=1, keepdims=True), 0.0)
     fs_send[...] = squares
     final_copies = tp_copies(6, lambda peer: fs_send, fs_recv.at[tp])
@@ -302,41 +570,27 @@
 ):
     tp_count = lax.axis_size("tp")
     ep_count = lax.axis_size("ep")
-    ep_place = lax.axis_index("ep")
     seqs, width = hidden.shape
     part = width // tp_count
     expert_gate, expert_up, expert_down, dense_gate, dense_up, dense_down = weights
     units = expert_gate.shape[2]
-    dense_units = dense_gate.shape[1]
+    dense_gate, dense_up = dense_gate.T, dense_up.T
+    dense_units = dense_gate.shape[0]
     top = routes.shape[1]
     experts = ep_count * expert_gate.shape[0]
     limit = 2 * seqs * top // ep_count
     capacity = -(-limit // 16) * 16
     rows_all = ep_count * seqs
+    rows_tp = rows_all // tp_count
+    groups = tp_count // 2
     f32, bf16 = jnp.float32, jnp.bfloat16
-    names = jnp.arange(experts, dtype=jnp.int32)
-    hits = routes[:, :, None] == names[None, None, :]
-    named = jnp.any(hits, axis=1)
-    order = jnp.arange(seqs, dtype=jnp.int32)
-    earlier = (order[None, :] < order[:, None])[:, :, None] & named[None, :, :]
-    rank = jnp.sum(earlier.astype(jnp.int32), axis=1)
-    code = jnp.where(named, rank + 1, 0).astype(f32)
-    block = jnp.arange(ep_count, dtype=jnp.int32)[None, :, None] == ep_place
-    codes = jnp.where(block, code.T[:, None, :], 0.0).reshape(experts, rows_all)
-    place = jnp.arange(capacity, dtype=jnp.int32)
-    combine = (
-        (hits.transpose(1, 0, 2)[:, :, :, None] & (rank[None, :, :, None] == place))
-        .astype(bf16)
-        .reshape(top * seqs, experts * capacity)
-    )
-    share = route_scores / jnp.sum(route_scores, axis=-1, keepdims=True)
     vmem = pl.BlockSpec(memory_space=pltpu.VMEM)
     hbm = pl.BlockSpec(memory_space=pl.ANY)
     slots = ep_count * capacity
     return pl.pallas_call(
         functools.partial(tail_kernel, tp_count, ep_count, capacity),
         out_shape=jax.ShapeDtypeStruct((seqs, part), bf16),
-        in_specs=[vmem] * 7 + [hbm] * 6,
+        in_specs=[vmem] * 6 + [hbm] * 6,
         out_specs=vmem,
         scratch_shapes=[
             pltpu.VMEM((width, units), bf16),
@@ -350,16 +604,21 @@
             pltpu.VMEM((tp_count, seqs, 128), f32),
             pltpu.VMEM((seqs, 128), f32),
             pltpu.VMEM((tp_count, seqs, 128), f32),
+            pltpu.VMEM((experts, rows_all), f32),
             pltpu.VMEM((ep_count, experts, rows_all), f32),
             pltpu.VMEM((rows_all, part), bf16),
             pltpu.VMEM((tp_count, slots, part), bf16),
             pltpu.VMEM((2, rows_all, dense_units), bf16),
-            pltpu.VMEM((tp_count, 2, rows_all // tp_count, dense_units), bf16),
+            pltpu.VMEM((groups, 2, rows_tp, dense_units), bf16),
+            pltpu.VMEM((groups, 2, rows_tp, dense_units), bf16),
+            pltpu.VMEM((groups, 2, rows_tp, dense_units), bf16),
             pltpu.VMEM((rows_all, dense_units), bf16),
             pltpu.VMEM((rows_all, part), bf16),
             pltpu.VMEM((ep_count, seqs, part), bf16),
             pltpu.VMEM((tp_count, slots, part), bf16),
-            pltpu.VMEM((tp_count, slots, part), bf16),
+            pltpu.VMEM((groups, slots, part), bf16),
+            pltpu.VMEM((groups, slots, part), bf16),
+            pltpu.VMEM((groups, slots, part), bf16),
             pltpu.VMEM((slots, part), bf16),
             pltpu.VMEM((slots, part), bf16),
             pltpu.SemaphoreType.DMA((6,)),
@@ -377,10 +636,14 @@
         hidden,
         norm_gains,
         dense_mix.reshape(1, width),
-        codes,
-        combine,
-        share,
-        *weights,
+        routes.T,
+        route_scores.T,
+        expert_gate,
+        expert_up,
+        expert_down,
+        dense_gate,
+        dense_up,
+        dense_down,
     )
 
 
@@ -408,47 +671,16 @@
     dense_down,
     dense_mix,
 ):
-    tp_place = lax.axis_index("tp")
-    seq_local, width = hidden.shape
-    heads_local = state_matrix.shape[1]
-    head_width = state_matrix.shape[2]
-    start_f = hidden.astype(jnp.float32)
-    normed_in = (
-        start_f
-        * lax.rsqrt(jnp.mean(start_f * start_f, axis=-1, keepdims=True) + EPS)
-        * norm_gains[0]
-    ).astype(jnp.bfloat16)
-    query_f = jnp.dot(normed_in, w_query, preferred_element_type=jnp.float32)
-    key_f = jnp.dot(normed_in, w_key, preferred_element_type=jnp.float32)
-    value_f = jnp.dot(normed_in, w_value, preferred_element_type=jnp.float32)
-    gate_f = jnp.dot(normed_in, w_outgate, preferred_element_type=jnp.float32)
-    head_first = tp_place * heads_local
-    input_weight = lax.dynamic_slice_in_dim(w_input_gate, head_first, heads_local, 1)
-    forget_weight = lax.dynamic_slice_in_dim(w_forget_gate, head_first, heads_local, 1)
-    forget_local = lax.dynamic_slice_in_dim(forget_bias, head_first, heads_local, 0)
-    in_gate = jnp.dot(normed_in, input_weight, preferred_element_type=jnp.float32)
-    log_forget = jax.nn.log_sigmoid(
-        jnp.dot(normed_in, forget_weight, preferred_element_type=jnp.float32) + forget_local
+    terms, new_matrix, new_norm, new_max = front(
+        hidden,
+        norm_gains,
+        (w_input_gate, w_forget_gate),
+        forget_bias,
+        state_norm,
+        state_max,
+        (w_query, w_key, w_value, w_outgate, w_mix_out),
+        state_matrix,
     )
-    query = settle(query_f).reshape(seq_local, heads_local, head_width)
-    keys = settle(key_f).reshape(seq_local, heads_local, head_width) * head_width ** (-0.5)
-    values = settle(value_f).reshape(seq_local, heads_local, head_width)
-    carried = log_forget + state_max
-    new_max = jnp.maximum(carried, in_gate)
-    keep = jnp.exp(carried - new_max)
-    write = jnp.exp(in_gate - new_max)
-    written = write[:, :, None] * keys
-    new_matrix = (
-        keep[:, :, None, None] * state_matrix + written[:, :, :, None] * values[:, :, None, :]
-    )
-    new_norm = keep[:, :, None] * state_norm + written
-    numer = jnp.einsum("shd,shdv->shv", query, new_matrix)
-    denom = jnp.einsum("shd,shd->sh", query, new_norm)
-    read = numer / jnp.maximum(jnp.abs(denom), jnp.exp(-new_max))[:, :, None]
-    mixed = (
-        jax.nn.sigmoid(settle(gate_f)) * read.reshape(seq_local, heads_local * head_width)
-    ).astype(jnp.bfloat16)
-    terms = jnp.dot(mixed, w_mix_out, preferred_element_type=jnp.float32).astype(jnp.bfloat16)
     new_hidden = tail(
         terms,
         hidden,

time: 84.1 us -> 71.1 us (0.85)
  matrix products: 11.4 us -> 0 us
  other arithmetic: 9.05 us -> 0 us
  local copies, waits for them, and re-layouts: 8.06 us -> 15.6 us
    dot_general x8 -> x0, matrix products: 11.4 us -> none  [the longest x1 2.97 us: local(): numer = jnp.einsum('shd,shdv->shv', query, new_matrix)]
    unnamed x18 -> x29, local copies, waits for them, and re-layouts: 4.94 us -> 15.6 us
    pallas_call x1, Pallas kernels: 54.3 us -> 47.5 us  [tail(): pl.pallas_call(functools.partial(tail_kernel, tp_count, ep_count, capacit...]
    pallas_call x0 -> x1, Pallas kernels: none -> 6.49 us  [front(): pl.pallas_call(front_kernel, out_shape=(jax.ShapeDtypeStruct((tp_count, s...]
    add x1 -> x0, other arithmetic: 4.32 us -> none  [local(): keep[:, :, None, None] * state_matrix]
    reduce_sum x3 -> x0, other arithmetic: 1.67 us -> none  [the longest x1 1.04 us: local(): jnp.mean(start_f * start_f, axis=-1, keepdims=True) + EPS]
    unnamed x1 -> x0, other arithmetic: 1.51 us -> none
    slice x1 -> x0, local copies, waits for them, and re-layouts: 0.85 us -> none  [local(): norm_gains[0]]
where the time goes in v2:
time: 71.1 us; the launch traced here: 70.3 us
  Pallas kernels  54 us (76%)
  local copies, waits for them, and re-layouts  15.6 us (22%)
    pallas_call x1, Pallas kernels, tail(): pl.pallas_call(functools.partial(tail_kernel, tp_count, ep_count, capacit...  47.5 us
    unnamed x29, local copies, waits for them, and re-layouts  15.6 us
    pallas_call x1, Pallas kernels, front(): pl.pallas_call(front_kernel, out_shape=(jax.ShapeDtypeStruct((tp_count, s...  6.49 us

profile of v2, /device:TPU:0, one launch (start us, length us, event | category | flops | bytes accessed | tf_op | source)
XLA Modules:
  0.0 70.3 jit_solution(3789009674958331358)
XLA Ops:
  0.6 0.0 copy-start
  0.6 2.2 %copy-done = f32[32,2,128,128]{3,2,1,0:T(8,128)S(1)} copy-done((f32[32,2,128,128]{3,2,1,0:T(8,128)S(1)}, f32[32,2,128,128]{3,2,1,0:T(8,128)}, u32[]{:S(2)}) %copy-start) | copy-done | bytes 4194328
  2.8 0.0 copy-start.1
  2.8 1.2 %copy-done.1 = bf16[2048,256]{1,0:T(8,128)(2,1)S(1)} copy-done((bf16[2048,256]{1,0:T(8,128)(2,1)S(1)}, bf16[2048,256]{1,0:T(8,128)(2,1)}, u32[]{:S(2)}) %copy-start.1) | copy-done | bytes 1048600
  4.0 0.0 copy-start.2
  4.1 1.2 %copy-done.2 = bf16[2048,256]{1,0:T(8,128)(2,1)S(1)} copy-done((bf16[2048,256]{1,0:T(8,128)(2,1)S(1)}, bf16[2048,256]{1,0:T(8,128)(2,1)}, u32[]{:S(2)}) %copy-start.2) | copy-done | bytes 1048600
  5.3 0.0 copy-start.3
  5.3 1.2 %copy-done.3 = bf16[2048,256]{1,0:T(8,128)(2,1)S(1)} copy-done((bf16[2048,256]{1,0:T(8,128)(2,1)S(1)}, bf16[2048,256]{1,0:T(8,128)(2,1)}, u32[]{:S(2)}) %copy-start.3) | copy-done | bytes 1048600
  6.5 0.0 copy-start.4
  6.5 1.2 %copy-done.4 = bf16[2048,256]{1,0:T(8,128)(2,1)S(1)} copy-done((bf16[2048,256]{1,0:T(8,128)(2,1)S(1)}, bf16[2048,256]{1,0:T(8,128)(2,1)}, u32[]{:S(2)}) %copy-start.4) | copy-done | bytes 1048600
  7.7 0.0 copy-start.5
  7.7 1.2 %copy-done.5 = bf16[256,2048]{1,0:T(8,128)(2,1)S(1)} copy-done((bf16[256,2048]{1,0:T(8,128)(2,1)S(1)}, bf16[256,2048]{1,0:T(8,128)(2,1)}, u32[]{:S(2)}) %copy-start.5) | copy-done | bytes 1048600
  9.0 0.9 %copy-done.6 = bf16[32,2048]{1,0:T(8,128)(2,1)S(1)} copy-done((bf16[32,2048]{1,0:T(8,128)(2,1)S(1)}, bf16[32,2048]{1,0:T(8,128)(2,1)}, u32[]{:S(2)}) %copy-start.6) | copy-done | bytes 131096
  9.9 0.8 %copy-done.8 = f32[4,2048]{1,0:T(4,128)S(1)} copy-done((f32[4,2048]{1,0:T(4,128)S(1)}, f32[4,2048]{1,0:T(4,128)}, u32[]{:S(2)}) %copy-start.8) | copy-done | bytes 32792
  10.6 0.8 %copy-done.9 = bf16[2048,8]{0,1:T(8,128)(2,1)S(1)} copy-done((bf16[2048,8]{0,1:T(8,128)(2,1)S(1)}, bf16[2048,8]{0,1:T(8,128)(2,1)}, u32[]{:S(2)}) %copy-start.9) | copy-done | bytes 32792
  11.4 0.8 %copy-done.10 = bf16[2048,8]{0,1:T(8,128)(2,1)S(1)} copy-done((bf16[2048,8]{0,1:T(8,128)(2,1)S(1)}, bf16[2048,8]{0,1:T(8,128)(2,1)}, u32[]{:S(2)}) %copy-start.10) | copy-done | bytes 32792
  12.1 0.8 %copy-done.11 = f32[32,2,128]{2,1,0:T(2,128)S(1)} copy-done((f32[32,2,128]{2,1,0:T(2,128)S(1)}, f32[32,2,128]{2,1,0:T(2,128)}, u32[]{:S(2)}) %copy-start.11) | copy-done | bytes 32792
  12.9 0.7 copy-done.12
  13.6 0.7 copy-done.13
  14.2 6.5 %front.1 = (bf16[4,32,512]{2,1,0:T(8,128)(2,1)S(1)}, f32[32,2,128,128]{3,2,1,0:T(8,128)}, f32[32,2,128]{2,1,0:T(2,128)}, f32[2,32]{1,0:T(2,128)}) custom-call(bf16[32,2048]{1,0:T(8,128)(2,1)S(1)} %copy-done.6, f32[4,2048]{1,0:T(4,128)S(1)} %copy-done.8, bf16[8,2048]{1,0:T(8,128)(2,1)S(1)} %bitcast.10, bf16[8,2048]{1,0:T(8,128)(2,1)S(1)} %bitcast.11, ...), custom_call_target="tpu_custom_call" | custom-call | tf_op jit(solution)/shard_map/front/pallas_call | solution.py:143
  20.7 0.0 copy-start.7
  20.7 0.6 copy-done.7
  21.4 47.5 %tail.1 = bf16[32,512]{1,0:T(8,128)(2,1)} custom-call(bf16[4,32,512]{2,1,0:T(8,128)(2,1)} %copy-done.7, bf16[32,2048]{1,0:T(8,128)(2,1)} %hidden_ref.3, f32[4,2048]{1,0:T(4,128)} %gains_ref.3, f32[1,2048]{1,0:T(1,128)} %bitcast.16, s32[2,32]{1,0:T(2,128)} %bitcast.17, f32[2,32]{1,0:T(2,128)} %bitcast.18, bf16[1,2048,896]{2,1,0:T(8,128)(2,1)} %eg_hbm.1, ...), custom_call_target="tpu_custom_call" | custom-call | tf_op jit(solution)/shard_map/tail/pallas_call | solution.py:590
  68.9 1.4 %copy.27 = bf16[32,512]{1,0:T(8,128)(2,1)} copy(bf16[32,512]{1,0:T(8,128)(2,1)} %tail.1) | data formatting | bytes 65536
  (7 shorter events, 0.0 us)
Async XLA Ops:
  0.6 2.2 %copy-start = (f32[32,2,128,128]{3,2,1,0:T(8,128)S(1)}, f32[32,2,128,128]{3,2,1,0:T(8,128)}, u32[]{:S(2)}) copy-start(f32[32,2,128,128]{3,2,1,0:T(8,128)} %state_hbm.1) | copy-start | bytes 12582916
  2.8 1.2 %copy-start.1 = (bf16[2048,256]{1,0:T(8,128)(2,1)S(1)}, bf16[2048,256]{1,0:T(8,128)(2,1)}, u32[]{:S(2)}) copy-start(bf16[2048,256]{1,0:T(8,128)(2,1)} %wq_hbm.1) | copy-start | bytes 3145732
  4.0 1.2 %copy-start.2 = (bf16[2048,256]{1,0:T(8,128)(2,1)S(1)}, bf16[2048,256]{1,0:T(8,128)(2,1)}, u32[]{:S(2)}) copy-start(bf16[2048,256]{1,0:T(8,128)(2,1)} %wk_hbm.1) | copy-start | bytes 3145732
  5.3 1.2 %copy-start.3 = (bf16[2048,256]{1,0:T(8,128)(2,1)S(1)}, bf16[2048,256]{1,0:T(8,128)(2,1)}, u32[]{:S(2)}) copy-start(bf16[2048,256]{1,0:T(8,128)(2,1)} %wv_hbm.1) | copy-start | bytes 3145732
  6.5 1.2 %copy-start.4 = (bf16[2048,256]{1,0:T(8,128)(2,1)S(1)}, bf16[2048,256]{1,0:T(8,128)(2,1)}, u32[]{:S(2)}) copy-start(bf16[2048,256]{1,0:T(8,128)(2,1)} %wo_hbm.1) | copy-start | bytes 3145732
  7.7 1.2 %copy-start.5 = (bf16[256,2048]{1,0:T(8,128)(2,1)S(1)}, bf16[256,2048]{1,0:T(8,128)(2,1)}, u32[]{:S(2)}) copy-start(bf16[256,2048]{1,0:T(8,128)(2,1)} %wm_hbm.1) | copy-start | bytes 3145732
  8.9 0.9 %copy-start.6 = (bf16[32,2048]{1,0:T(8,128)(2,1)S(1)}, bf16[32,2048]{1,0:T(8,128)(2,1)}, u32[]{:S(2)}) copy-start(bf16[32,2048]{1,0:T(8,128)(2,1)} %hidden_ref.3) | copy-start | bytes 393220
  9.9 0.8 %copy-start.8 = (f32[4,2048]{1,0:T(4,128)S(1)}, f32[4,2048]{1,0:T(4,128)}, u32[]{:S(2)}) copy-start(f32[4,2048]{1,0:T(4,128)} %gains_ref.3) | copy-start | bytes 98308
  10.6 0.8 %copy-start.9 = (bf16[2048,8]{0,1:T(8,128)(2,1)S(1)}, bf16[2048,8]{0,1:T(8,128)(2,1)}, u32[]{:S(2)}) copy-start(bf16[2048,8]{0,1:T(8,128)(2,1)} %param.28) | copy-start | bytes 98308
  11.4 0.8 %copy-start.10 = (bf16[2048,8]{0,1:T(8,128)(2,1)S(1)}, bf16[2048,8]{0,1:T(8,128)(2,1)}, u32[]{:S(2)}) copy-start(bf16[2048,8]{0,1:T(8,128)(2,1)} %param.29) | copy-start | bytes 98308
  12.1 0.8 %copy-start.11 = (f32[32,2,128]{2,1,0:T(2,128)S(1)}, f32[32,2,128]{2,1,0:T(2,128)}, u32[]{:S(2)}) copy-start(f32[32,2,128]{2,1,0:T(2,128)} %norm_ref.1) | copy-start | bytes 98308
  12.9 0.7 copy-start.12
  13.6 0.7 copy-start.13
  20.7 0.7 copy-start.7

commit v3 on v2

--- a/solution.py
+++ b/solution.py
@@ -158,7 +158,7 @@
             pltpu.SemaphoreType.DMA((chunks,)),
             pltpu.SemaphoreType.DMA((chunks,)),
         ],
-        compiler_params=pltpu.CompilerParams(vmem_limit_bytes=40 * 1024 * 1024),
+        compiler_params=pltpu.CompilerParams(vmem_limit_bytes=67043328),
         name="front",
     )(
         hidden,
@@ -628,7 +628,7 @@
             pltpu.SemaphoreType.DMA((4, ep_count - 1)),
         ],
         compiler_params=pltpu.CompilerParams(
-            collective_id=0, has_side_effects=True, vmem_limit_bytes=56 * 1024 * 1024
+            collective_id=0, has_side_effects=True, vmem_limit_bytes=67043328
         ),
         name="tail",
     )(

time: 71.1 us -> 57.8 us (0.81)
  local copies, waits for them, and re-layouts: 15.6 us -> 1.38 us
  Pallas kernels: 54 us -> 55.5 us
    unnamed x29 -> x1, local copies, waits for them, and re-layouts: 15.6 us -> 1.38 us
    pallas_call x1, Pallas kernels: 6.49 us -> 7.98 us  [front(): pl.pallas_call(front_kernel, out_shape=(jax.ShapeDtypeStruct((tp_count, s...]
where the time goes in v3:
time: 57.8 us; the launch traced here: 57.6 us
  Pallas kernels  55.5 us (96%)
  local copies, waits for them, and re-layouts  1.38 us (2%)
  between operations  0.65 us (1%)
    pallas_call x1, Pallas kernels, tail(): pl.pallas_call(functools.partial(tail_kernel, tp_count, ep_count, capacit...  47.5 us
    pallas_call x1, Pallas kernels, front(): pl.pallas_call(front_kernel, out_shape=(jax.ShapeDtypeStruct((tp_count, s...  7.98 us
    unnamed x1, local copies, waits for them, and re-layouts  1.38 us

profile of v3, /device:TPU:0, one launch (start us, length us, event | category | flops | bytes accessed | tf_op | source)
XLA Modules:
  0.0 57.6 jit_solution(3262366959568186824)
XLA Ops:
  0.6 8.0 %front.1 = (bf16[4,32,512]{2,1,0:T(8,128)(2,1)}, f32[32,2,128,128]{3,2,1,0:T(8,128)}, f32[32,2,128]{2,1,0:T(2,128)}, f32[2,32]{1,0:T(2,128)}) custom-call(bf16[32,2048]{1,0:T(8,128)(2,1)} %hidden_ref.3, f32[4,2048]{1,0:T(4,128)} %gains_ref.3, bf16[8,2048]{1,0:T(8,128)(2,1)} %bitcast.12, bf16[8,2048]{1,0:T(8,128)(2,1)} %bitcast.13, f32[1,8]{1,0:T(1,128)} %bitcast.18, ...), custom_call_target="tpu_custom_call" | custom-call | tf_op jit(solution)/shard_map/front/pallas_call | solution.py:143
  8.6 47.5 %tail.1 = bf16[32,512]{1,0:T(8,128)(2,1)} custom-call(bf16[4,32,512]{2,1,0:T(8,128)(2,1)} %get-tuple-element.8.terms_ref, bf16[32,2048]{1,0:T(8,128)(2,1)} %hidden_ref.3, f32[4,2048]{1,0:T(4,128)} %gains_ref.3, f32[1,2048]{1,0:T(1,128)} %bitcast.14, s32[2,32]{1,0:T(2,128)} %bitcast.16, f32[2,32]{1,0:T(2,128)} %bitcast.17, bf16[1,2048,896]{2,1,0:T(8,128)(2,1)} %eg_hbm.1, ...), custom_call_target="tpu_custom_call" | custom-call | tf_op jit(solution)/shard_map/tail/pallas_call | solution.py:590
  56.2 1.4 %copy.27 = bf16[32,512]{1,0:T(8,128)(2,1)} copy(bf16[32,512]{1,0:T(8,128)(2,1)} %tail.1) | data formatting | bytes 65536
